TPU v7x, 256 devices: a whole 4x4x8 slice. The times are simulated.
256 devices in a mesh: ep: 64 (over z, y, core), tp: 4 (over x).
Axes of the slice: x: 4, y: 4, z: 8, core: 2. Of those that a mesh axis runs over, the one named last changes fastest.
Arguments:
- queries: bfloat16 [8192, 512], P('ep', 'tp'), may hold values from -8 to 8
- key_cache: bfloat16 [4, 64, 8192], P('tp', None, 'ep'), may hold values from -4.5 to 4.5
- value_cache: bfloat16 [4, 64, 8192], P('tp', None, 'ep'), may hold values from -6 to 6
- cum_gate: float32 [4, 8192], P('tp'), may hold values from -2048 to 0, as said below
- out_weight: bfloat16 [512, 2048], replicated, may hold values from -1 to 1
- routed_input: bfloat16 [16384, 2048], P('ep'), may hold values from -6 to 6
- norm_gain: bfloat16 [2048], replicated, may hold values from 0.099609375 to 1.8984375
- routes: int32 [16384, 2], P('ep'), may hold values from 0 to 63, all different within a row; in each aligned block of 64 rows (0 to 63, 64 to 127, ...) at most 3 rows name the same one
- route_weight: float32 [16384, 2], P('ep'), may hold values from 0.2 to 1
- expert_gate: bfloat16 [64, 2048, 1024], P('ep', None, 'tp'), may hold values from -0.125 to 0.125
- expert_up: bfloat16 [64, 2048, 1024], P('ep', None, 'tp'), may hold values from -0.125 to 0.125
- expert_down: bfloat16 [64, 1024, 2048], P('ep', 'tp'), may hold values from -0.1875 to 0.1875
Outputs:
- mixed_out: bfloat16 [8192, 2048], P(('ep', 'tp'))
- expert_out: bfloat16 [16384, 2048], P(('ep', 'tp'))
Inputs may be any that keep to these rules, and one draw needn't show every extreme that they name: `cum_gate`: Non-increasing along positions in every head. `routes`: each row names 2 different experts. In each aligned block of 64 rows (the rows of one device) no expert is named by more than 3 rows, a bound that some block reaches.
All inputs are finite; a program needn't handle non-finite values.
Results may differ from a plain program's by a relative error of at most 0.012.
Values may be sent and summed in bfloat16 or wider, within the bound.
No kernel may reach another device: no remote copies, remote signals or barrier semaphores. Data moves between devices by JAX's collectives and lax.ppermute only.
A program may use at most 64 MiB of HBM per device.

v0:
```python
import jax
import jax.numpy as jnp
from jax import lax
from jax.sharding import PartitionSpec as P


def side_by_side(arrays, axis, dim, along):
    both = jnp.concatenate(arrays, axis=along)
    out, at, gathered = (lax.all_gather(both, axis, axis=dim, tiled=True), 0, [])
    for a in arrays:
        gathered.append(lax.slice_in_dim(out, at, at + a.shape[along], axis=along))
        at += a.shape[along]
    return tuple(gathered)


def joined_along(parts, dim):
    lengths = list(parts.shape[1:])
    lengths[dim] *= parts.shape[0]
    return jnp.moveaxis(parts, 0, dim).reshape(lengths)


def copy_for_each(x, axis):
    count = lax.axis_size(axis)
    return lax.all_to_all(jnp.broadcast_to(x[None], (count, *x.shape)), axis, 0, 0, tiled=True)


def gather_directly(x, axis, dim):
    return joined_along(copy_for_each(x, axis), dim)


def in_blocks(x, dim, count):
    before, after = (x.shape[:dim], x.shape[dim + 1 :])
    return jnp.moveaxis(x.reshape(*before, count, -1, *after), dim, 0)


def sum_at_owner(x, axis, dim):
    count = lax.axis_size(axis)
    parts = lax.all_to_all(in_blocks(x, dim, count), axis, 0, 0, tiled=True)
    return jnp.sum(parts.astype(jnp.float32), axis=0)


def slot_chooser(route_rows, expert_count, capacity):
    token_rows, top_count = route_rows.shape
    flat = route_rows.reshape(token_rows * top_count)
    same = (flat[:, None] == jnp.arange(expert_count, dtype=jnp.int32)[None, :]).astype(jnp.int32)
    earlier = jnp.cumsum(same, axis=0) - same
    rank = jnp.sum(earlier * same, axis=1)
    slot = flat * capacity + rank
    chosen = slot[:, None] == jnp.arange(expert_count * capacity, dtype=jnp.int32)[None, :]
    return chosen.astype(jnp.bfloat16).reshape(token_rows, top_count, expert_count * capacity)


def rms_rows(source, norm_gain):
    widened = source.astype(jnp.float32)
    scale = lax.rsqrt(jnp.mean(widened * widened, axis=-1, keepdims=True) + 1e-06)
    return (widened * scale * norm_gain.astype(jnp.float32)).astype(jnp.bfloat16)


def mixer_half(queries, key_cache, value_cache, cum_gate, out_weight):
    seq_rows = queries.shape[0]
    local_heads = key_cache.shape[0]
    head_size = key_cache.shape[1]
    group = queries.shape[1] // (local_heads * head_size)
    own_start = lax.axis_index("ep") * seq_rows
    query_heads = queries.reshape(seq_rows, local_heads, group, head_size)
    query_pos = own_start + jnp.arange(seq_rows, dtype=jnp.int32)
    gate_query = lax.dynamic_slice_in_dim(cum_gate, own_start, seq_rows, 1)
    gate_rows = jnp.transpose(gate_query)[:, :, None, None]
    scale = head_size ** (-0.5)
    best_start = jnp.full((seq_rows, local_heads, group), -jnp.inf, jnp.float32)
    total_start = jnp.zeros((seq_rows, local_heads, group), jnp.float32)
    summed_start = jnp.zeros((seq_rows, local_heads * group * head_size), jnp.float32)
    pieces = side_by_side((key_cache, value_cache), "ep", 2, 0)

    def update(state):
        best, total, summed = state
        key_piece, value_piece = pieces
        width = key_piece.shape[2]
        scores = (
            jnp.einsum("thgd,hds->thgs", query_heads, key_piece, preferred_element_type=jnp.float32)
            * scale
        )
        scores = scores + gate_rows - cum_gate[None, :, None, :]
        key_pos = jnp.arange(width, dtype=jnp.int32)
        allowed = key_pos[None, :] <= query_pos[:, None]
        scores = jnp.where(allowed[:, None, None, :], scores, -jnp.inf)
        new_best = jnp.max(scores, axis=-1)
        factor = jnp.exp(best - new_best)
        weights = jnp.exp(scores - new_best[..., None])
        new_total = total * factor + jnp.sum(weights, axis=-1)
        product = jnp.einsum(
            "thgs,hds->thgd",
            weights.astype(jnp.bfloat16),
            value_piece,
            preferred_element_type=jnp.float32,
        )
        new_summed = summed.reshape(product.shape) * factor[..., None] + product
        return (new_best, new_total, new_summed.reshape(seq_rows, local_heads * group * head_size))

    best, total, summed = lax.cond(
        jnp.int32(0) <= own_start,
        update,
        lambda state: state,
        (best_start, total_start, summed_start),
    )
    attended = summed.reshape(seq_rows, local_heads, group, head_size) / total[..., None]
    attended = attended.astype(jnp.bfloat16).reshape(seq_rows, local_heads * group * head_size)
    by_position = lax.all_to_all(attended, "tp", split_axis=0, concat_axis=1, tiled=True)
    return jnp.dot(by_position, out_weight, preferred_element_type=jnp.float32).astype(jnp.bfloat16)


def expert_half(routed_input, norm_gain, routes, route_weight, expert_gate, expert_up, expert_down):
    group_size = lax.axis_size("tp")
    ep_size = lax.axis_size("ep")
    tp_index = lax.axis_index("tp")
    seq_rows, width = routed_input.shape
    own_rows = seq_rows // group_size
    local_experts = expert_gate.shape[0]
    expert_count = local_experts * ep_size
    top_count = routes.shape[1]
    capacity = max(2, own_rows * top_count * 3 // (2 * expert_count))
    per_device = local_experts * capacity

    def hidden_units(received):
        blocks = received.shape[0]
        divide_point = received.reshape(blocks, ep_size, local_experts, capacity, width)
        gate = jnp.einsum(
            "abecd,edf->abecf", divide_point, expert_gate, preferred_element_type=jnp.float32
        )
        upper = jnp.einsum(
            "abecd,edf->abecf", divide_point, expert_up, preferred_element_type=jnp.float32
        )
        return (jax.nn.silu(gate) * upper).astype(jnp.bfloat16)

    mine = lax.dynamic_slice_in_dim(routed_input, tp_index * own_rows, own_rows, 0)
    own_routes = lax.dynamic_slice_in_dim(routes, tp_index * own_rows, own_rows, 0)
    chooser = slot_chooser(own_routes, expert_count, capacity)
    normed = rms_rows(mine, norm_gain)
    outgoing = jnp.einsum("tks,td->sd", chooser, normed, preferred_element_type=jnp.float32).astype(
        jnp.bfloat16
    )
    arrived = lax.all_to_all(
        outgoing.reshape(1, ep_size, per_device, width),
        "ep",
        split_axis=1,
        concat_axis=1,
        tiled=True,
    )
    hidden = (lambda piece, start: hidden_units(piece))(
        gather_directly(arrived, "tp", 0), jnp.int32(0)
    )
    partial_value = jnp.einsum(
        "abecf,efd->abecd", hidden, expert_down, preferred_element_type=jnp.float32
    )
    rounded = lax.optimization_barrier(partial_value.astype(jnp.bfloat16)).astype(jnp.float32)
    summed = sum_at_owner(
        rounded.reshape(1 * lax.axis_size("tp"), ep_size, per_device, width).astype(jnp.bfloat16),
        "tp",
        0,
    )
    returned = lax.all_to_all(
        summed.astype(jnp.bfloat16), "ep", split_axis=1, concat_axis=1, tiled=True
    )
    picked = jnp.einsum(
        "tks,sd->tkd",
        chooser,
        returned.reshape(ep_size * per_device, width),
        preferred_element_type=jnp.float32,
    )
    own_weight = lax.dynamic_slice_in_dim(route_weight, tp_index * own_rows, own_rows, 0)
    return jnp.sum(own_weight[:, :, None] * picked, axis=1).astype(jnp.bfloat16)


def body(
    queries,
    key_cache,
    value_cache,
    cum_gate,
    out_weight,
    routed_input,
    norm_gain,
    routes,
    route_weight,
    expert_gate,
    expert_up,
    expert_down,
):
    mixed_out = mixer_half(queries, key_cache, value_cache, cum_gate, out_weight)
    expert_out = expert_half(
        routed_input, norm_gain, routes, route_weight, expert_gate, expert_up, expert_down
    )
    return (mixed_out, expert_out)


def solution(mesh):
    return jax.shard_map(
        body,
        mesh=mesh,
        in_specs=(
            P("ep", "tp"),
            P("tp", None, "ep"),
            P("tp", None, "ep"),
            P("tp", None),
            P(),
            P("ep", None),
            P(),
            P("ep", None),
            P("ep", None),
            P("ep", None, "tp"),
            P("ep", None, "tp"),
            P("ep", "tp", None),
        ),
        out_specs=(P(("ep", "tp"), None), P(("ep", "tp"), None)),
        check_vma=False,
    )
```

profile of v0, /device:TPU:1, one launch (start us, length us, event | category | flops | bytes accessed | tf_op | source)
XLA Modules:
  0.0 209.8 jit_solution(6337569638874446934)
XLA Ops:
  7.2 0.0 copy-start
  7.2 0.9 constant_dynamic-slice_fusion
  8.1 0.1 copy.63
  8.2 0.1 eq.51
  8.3 0.1 fusion.62
  8.4 0.2 reduce_window_sum.11
  8.6 0.2 select_reduce_fusion
  8.8 0.1 reduce_sum.62
  8.9 0.1 copy.64
  9.0 0.8 multiply_add_fusion
  9.8 0.1 convert_reduce_fusion
  9.9 0.7 convert_element_type.77
  10.5 1.1 fusion.49
  11.7 2.3 %convolution_convert_fusion.1 = bf16[192,2048]{1,0:T(8,128)(2,1)} fusion(bf16[64,192]{1,0:T(8,128)(2,1)S(1)} %convert_reduce_fusion, f32[2048]{0:T(1024)S(1)} %convert_element_type.77, f32[64]{0:T(128)S(1)} %add_rsqrt_fusion, bf16[256,2048]{1,0:T(8,128)(2,1)} %param.19, s32[]{:T(128)S(6)} %select_n.15), kind=kOutput, calls=%fused_computation.30 | convolution fusion | flops 50855936 | bytes 1081604 | tf_op jit(solution)/shard_map/tks,td->sd/dot_general | solution.py:139
  13.9 2.4 %reshape.234 = bf16[1,64,3,2048]{3,2,1,0:T(4,128)(2,1)S(1)} reshape(bf16[192,2048]{1,0:T(8,128)(2,1)} %convolution_convert_fusion.1) | data formatting | bytes 1572864 | tf_op jit(solution)/shard_map/reshape | solution.py:143
  16.4 41.1 %all_to_all.39 = bf16[1,64,3,2048]{3,2,0,1:T(4,128)(2,1)S(1)} all-to-all(bf16[1,64,3,2048]{3,2,0,1:T(4,128)(2,1)S(1)} %bitcast.147), channel_id=1, replica_groups=mesh['ep'=64,'tp'=4] {'ep'}, dimensions={1} | all-to-all | bytes 1572864 | tf_op jit(solution)/shard_map/all_to_all | solution.py:142
  57.5 0.6 copy.66
  58.1 0.0 copy-start.3
  58.1 0.0 copy-start.4
  58.1 2.1 broadcast_in_dim.37
  60.2 4.6 %all-to-all-start.2 = ((bf16[4,1,64,3,2048]{4,2,3,1,0:T(8,128)(2,1)}), bf16[4,1,64,3,2048]{4,2,3,1,0:T(8,128)(2,1)}, u32[]{:S(2)}, u32[]{:S(2)}) async-start(bf16[4,1,64,3,2048]{4,2,3,1,0:T(8,128)(2,1)} %broadcast_in_dim.37), calls=%async_computation.2 | async-start | bytes 6291456 | tf_op jit(solution)/shard_map/all_to_all | solution.py:24
  64.8 0.0 all-gather.2.cloned.1.call-start
  64.9 0.6 pad_maximum_fusion
  65.5 0.0 all-gather.2.cloned.1.call-update
  65.5 35.8 %all-to-all-done.2 = bf16[4,1,64,3,2048]{4,2,3,1,0:T(8,128)(2,1)} async-done(((bf16[4,1,64,3,2048]{4,2,3,1,0:T(8,128)(2,1)}), bf16[4,1,64,3,2048]{4,2,3,1,0:T(8,128)(2,1)}, u32[]{:S(2)}, u32[]{:S(2)}) %all-to-all-start.2) | async-done | bytes 3145760 | tf_op jit(solution)/shard_map/all_to_all | solution.py:24
  101.4 3.8 %fusion.26 = f32[4,64,1,3,256]{4,1,3,0,2:T(8,128)} fusion(bf16[4,1,64,3,2048]{4,2,3,1,0:T(8,128)(2,1)} %all-to-all-done.2, bf16[1,2048,256]{2,1,0:T(8,128)(2,1)S(1)} %copy-done.6), kind=kOutput, calls=%fused_computation.33 | convolution fusion | flops 805306368 | bytes 4980736 | tf_op jit(solution)/shard_map/abecd,edf->abecf/dot_general | solution.py:127
  105.2 7.7 %fusion.25 = bf16[4,64,1,3,2048]{4,1,3,0,2:T(8,128)(2,1)} fusion(bf16[1,256,2048]{2,1,0:T(8,128)(2,1)} %param.25, bf16[4,1,64,3,2048]{4,2,3,1,0:T(8,128)(2,1)} %all-to-all-done.2, bf16[1,2048,256]{2,1,0:T(8,128)(2,1)} %param.24, f32[4,64,1,3,256]{4,1,3,0,2:T(8,128)} %fusion.26), kind=kOutput, calls=%fused_computation.29 | convolution fusion | flops 1613365248 | bytes 9175040 | tf_op jit(solution)/shard_map/abecf,efd->abecd/dot_general | solution.py:152
  112.9 4.8 %all-to-all-start.3 = ((bf16[4,1,64,3,2048]{4,2,3,1,0:T(8,128)(2,1)}), bf16[4,1,64,3,2048]{4,2,3,1,0:T(8,128)(2,1)}, u32[]{:S(2)}, u32[]{:S(2)}) async-start(bf16[4,1,64,3,2048]{4,2,3,1,0:T(8,128)(2,1)} %bitcast.149), calls=%async_computation.3 | async-start | bytes 6291456 | tf_op jit(solution)/shard_map/all_to_all | solution.py:38
  117.7 21.0 %all-gather.2.cloned.1.call-done = bf16[2,64,8192]{2,1,0:T(8,128)(2,1)} async-done(((bf16[2,64,128]{2,1,0:T(8,128)(2,1)}), bf16[2,64,8192]{2,1,0:T(8,128)(2,1)}) %all-gather.2.cloned.1.call-update) | async-done | bytes 2097168 | tf_op jit(solution)/shard_map/all_gather | solution.py:9
  138.7 7.7 %conditional.1 = (f32[128,1,2]{0,2,1:T(2,128)S(1)}, f32[128,128]{0,1:T(8,128)S(1)}) conditional(s32[]{:T(128)} %convert_element_type.70, () %tuple.19, (s32[]{:T(128)}, s32[128]{0:T(128)S(1)}, bf16[2,64,8192]{2,1,0:T(8,128)(2,1)}, bf16[128,128]{1,0:T(8,128)(2,1)S(1)}, f32[1,8192]{1,0:T(1,128)S(1)}) %tuple.35), branch_computations={%region_0.0_spmd, %region_1.4_spmd} | conditional | flops 556810624 | bytes 37957720 | solution.py:100
  138.7 0.1 dynamic-slice_bitcast_fusion
  138.7 0.1 copy.60
  138.9 0.7 iota_compare_fusion
  139.6 3.8 %fusion.67 = (f32[128,2]{0,1:T(2,128)S(1)}, f32[128,1,2,8192]{0,3,2,1:T(8,128)S(1)}) fusion(f32[8192]{0:T(1024)S(1)} %bitcast.154, f32[128]{0:T(128)S(1)} %dynamic-slice_bitcast_fusion, bf16[128,2,64]{0,2,1:T(8,128)(2,1)S(1)} %bitcast.152, bf16[2,64,8192]{2,1,0:T(8,128)(2,1)} %get-tuple-element.52, pred[128,8192]{0,1:T(8,128)(4,1)S(1)} %iota_compare_fusion), kind=kOutput, calls=%fused_computation.71 | convolution fusion | flops 278920960 | bytes 10552832 | tf_op jit(solution)/shard_map/cond/branch_1_fun/thgd,hds->thgs/dot_general | solution.py:80
  143.4 1.1 fusion.6
  144.5 0.5 copy-done.1
  145.0 1.4 fusion.14
  146.4 0.7 copy.61
  147.2 6.2 %all-to-all-done.3 = bf16[4,1,64,3,2048]{4,2,3,1,0:T(8,128)(2,1)} async-done(((bf16[4,1,64,3,2048]{4,2,3,1,0:T(8,128)(2,1)}), bf16[4,1,64,3,2048]{4,2,3,1,0:T(8,128)(2,1)}, u32[]{:S(2)}, u32[]{:S(2)}) %all-to-all-start.3) | async-done | bytes 3145760 | tf_op jit(solution)/shard_map/all_to_all | solution.py:38
  153.4 3.4 %all-to-all-start = ((bf16[4,32,128]{2,1,0:T(8,128)(2,1)}), bf16[4,32,128]{2,1,0:T(8,128)(2,1)S(1)}, u32[]{:S(2)}, u32[]{:S(2)}) async-start(bf16[4,32,128]{2,1,0:T(8,128)(2,1)} %bitcast.17), calls=%async_computation | async-start | bytes 65536 | tf_op jit(solution)/shard_map/all_to_all | solution.py:108
  156.9 2.5 %bitcast_reduce_fusion = bf16[64,3,2048]{2,0,1:T(8,128)(2,1)S(1)} fusion(bf16[4,1,64,3,2048]{4,2,3,1,0:T(8,128)(2,1)} %all-to-all-done.3), kind=kLoop, calls=%fused_computation.24 | loop fusion | flops 1179648 | bytes 3932160 | tf_op jit(solution)/shard_map/reduce_sum | solution.py:39
  159.3 1.7 copy.69
  161.0 10.1 %all-to-all-start.4 = ((bf16[1,64,3,2048]{3,2,0,1:T(4,128)(2,1)}), bf16[1,64,3,2048]{3,2,0,1:T(4,128)(2,1)S(1)}, u32[]{:S(2)}, u32[]{:S(2)}) async-start(bf16[1,64,3,2048]{3,2,0,1:T(4,128)(2,1)} %copy.69), calls=%async_computation.4 | async-start | bytes 2097152 | tf_op jit(solution)/shard_map/all_to_all | solution.py:161
  171.1 0.1 constant_dynamic-slice_fusion.1
  171.2 1.1 convolution_convert_fusion.2
  172.3 26.9 %all-to-all-done.4 = bf16[1,64,3,2048]{3,2,0,1:T(4,128)(2,1)S(1)} async-done(((bf16[1,64,3,2048]{3,2,0,1:T(4,128)(2,1)}), bf16[1,64,3,2048]{3,2,0,1:T(4,128)(2,1)S(1)}, u32[]{:S(2)}, u32[]{:S(2)}) %all-to-all-start.4) | async-done | bytes 786464 | tf_op jit(solution)/shard_map/all_to_all | solution.py:161
  199.3 1.4 reshape.246
  200.7 2.3 %fusion.35 = bf16[64,2048]{1,0:T(8,128)(2,1)} fusion(bf16[192,2048,1]{1,0,2:T(8,128)(2,1)} %reshape.246, f32[64,2]{0,1:T(2,128)S(1)} %constant_dynamic-slice_fusion.1, s32[64,2]{0,1:T(2,128)S(1)} %multiply_add_fusion), kind=kOutput, calls=%fused_computation.36 | convolution fusion | flops 101081088 | bytes 1049600 | tf_op jit(solution)/shard_map/tks,sd->tkd/dot_general | solution.py:164
  (18 shorter events, 0.1 us)
Async XLA Ops:
  7.2 164.0 %copy-start = (bf16[512,2048]{1,0:T(8,128)(2,1)S(1)}, bf16[512,2048]{1,0:T(8,128)(2,1)}, u32[]{:S(2)}) copy-start(bf16[512,2048]{1,0:T(8,128)(2,1)} %param.18) | copy-start | bytes 6291460
  58.1 6.8 %copy-start.3 = (bf16[1,64,128]{2,1,0:T(8,128)(2,1)S(1)}, bf16[1,64,128]{2,1,0:T(8,128)(2,1)}, u32[]{:S(2)}) copy-start(bf16[1,64,128]{2,1,0:T(8,128)(2,1)} %param.16) | copy-start | bytes 49156
  58.1 6.8 %copy-start.4 = (bf16[1,64,128]{2,1,0:T(8,128)(2,1)S(1)}, bf16[1,64,128]{2,1,0:T(8,128)(2,1)}, u32[]{:S(2)}) copy-start(bf16[1,64,128]{2,1,0:T(8,128)(2,1)} %param.15) | copy-start | bytes 49156
  58.1 43.3 %copy-start.6 = (bf16[1,2048,256]{2,1,0:T(8,128)(2,1)S(1)}, bf16[1,2048,256]{2,1,0:T(8,128)(2,1)}, u32[]{:S(2)}) copy-start(bf16[1,2048,256]{2,1,0:T(8,128)(2,1)} %param.23) | copy-start | bytes 3145732
  60.2 41.2 %all-to-all-start.2 = ((bf16[4,1,64,3,2048]{4,2,3,1,0:T(8,128)(2,1)}), bf16[4,1,64,3,2048]{4,2,3,1,0:T(8,128)(2,1)}, u32[]{:S(2)}, u32[]{:S(2)}) async-start(bf16[4,1,64,3,2048]{4,2,3,1,0:T(8,128)(2,1)} %broadcast_in_dim.37), calls=%async_computation.2 | async-start | bytes 6291456 | tf_op jit(solution)/shard_map/all_to_all | solution.py:24
  64.8 73.9 %all-gather.2.cloned.1.call-start = ((), (), s32[]{:S(2)}) async-start(), calls=%async_computation.5 | async-start | bytes 2129920 | tf_op jit(solution)/shard_map/all_gather | solution.py:9
  112.9 25.8 %copy-start.2 = (bf16[128,128]{1,0:T(8,128)(2,1)S(1)}, bf16[128,128]{1,0:T(8,128)(2,1)}, u32[]{:S(2)}) copy-start(bf16[128,128]{1,0:T(8,128)(2,1)} %param.14) | copy-start | bytes 98308
  112.9 25.8 %copy-start.7 = (f32[1,8192]{1,0:T(1,128)S(1)}, f32[1,8192]{1,0:T(1,128)}, u32[]{:S(2)}) copy-start(f32[1,8192]{1,0:T(1,128)} %param.17) | copy-start | bytes 98308
  112.9 40.5 %all-to-all-start.3 = ((bf16[4,1,64,3,2048]{4,2,3,1,0:T(8,128)(2,1)}), bf16[4,1,64,3,2048]{4,2,3,1,0:T(8,128)(2,1)}, u32[]{:S(2)}, u32[]{:S(2)}) async-start(bf16[4,1,64,3,2048]{4,2,3,1,0:T(8,128)(2,1)} %bitcast.149), calls=%async_computation.3 | async-start | bytes 6291456 | tf_op jit(solution)/shard_map/all_to_all | solution.py:38
  143.4 1.6 copy-start.1
  146.4 24.7 %copy-start.5 = (f32[256,2]{0,1:T(2,128)S(1)}, f32[256,2]{0,1:T(2,128)}, u32[]{:S(2)}) copy-start(f32[256,2]{0,1:T(2,128)} %param.22) | copy-start | bytes 6148
  153.4 7.6 %all-to-all-start = ((bf16[4,32,128]{2,1,0:T(8,128)(2,1)}), bf16[4,32,128]{2,1,0:T(8,128)(2,1)S(1)}, u32[]{:S(2)}, u32[]{:S(2)}) async-start(bf16[4,32,128]{2,1,0:T(8,128)(2,1)} %bitcast.17), calls=%async_computation | async-start | bytes 65536 | tf_op jit(solution)/shard_map/all_to_all | solution.py:108
  161.0 38.3 %all-to-all-start.4 = ((bf16[1,64,3,2048]{3,2,0,1:T(4,128)(2,1)}), bf16[1,64,3,2048]{3,2,0,1:T(4,128)(2,1)S(1)}, u32[]{:S(2)}, u32[]{:S(2)}) async-start(bf16[1,64,3,2048]{3,2,0,1:T(4,128)(2,1)} %copy.69), calls=%async_computation.4 | async-start | bytes 2097152 | tf_op jit(solution)/shard_map/all_to_all | solution.py:161
Sparse Core Ops, SparseCore 0:
  68.8 69.7 all-gather.1
where the time goes:
time: 211 us; the launch traced here: 210 us
  waiting for transfers between devices  90 us (43%)
  blocking collectives  41.1 us (19%)
  starting transfers between devices  23 us (11%)
  matrix products  22.4 us (11%)
  between operations  14.2 us (7%)
  local copies, waits for them, and re-layouts  11 us (5%)
  other arithmetic  7.98 us (4%)
    all_to_all x1, blocking collectives, expert_half(): lax.all_to_all(outgoing.reshape(1, ep_size, per_device, width), 'ep', spl...  41.1 us
    all_to_all x1, waiting for transfers between devices, copy_for_each(): lax.all_to_all(jnp.broadcast_to(x[None], (count, *x.shape)), axis, 0, 0,...  35.8 us
    all_to_all x1, waiting for transfers between devices, expert_half(): lax.all_to_all(summed.astype(jnp.bfloat16), 'ep', split_axis=1, concat_ax...  26.9 us
    all_gather x1, waiting for transfers between devices, side_by_side(): lax.all_gather(both, axis, axis=dim, tiled=True)  21 us
    all_to_all x1, starting transfers between devices, expert_half(): lax.all_to_all(summed.astype(jnp.bfloat16), 'ep', split_axis=1, concat_ax...  10.1 us
    dot_general x1, matrix products, expert_half(): jnp.einsum('abecf,efd->abecd', hidden, expert_down, preferred_element_typ...  7.72 us
    all_to_all x1, waiting for transfers between devices, sum_at_owner(): parts = lax.all_to_all(in_blocks(x, dim, count), axis, 0, 0, tiled=True)  6.25 us
    all_to_all x1, starting transfers between devices, sum_at_owner(): parts = lax.all_to_all(in_blocks(x, dim, count), axis, 0, 0, tiled=True)  4.77 us
  transfers between devices with their start and end apart: 5, of which 4 were waited for; matrix products, arithmetic and copies ran while one was open for 12% of the time, Pallas kernels for 0%

commit v1 on v0

v1 whole, which is shorter than its diff:
```python
import jax
import jax.numpy as jnp
from jax import lax
from jax.experimental import pallas as pl
from jax.experimental.pallas import tpu as pltpu
from jax.sharding import PartitionSpec as P


Z, Y, C = 8, 4, 2
TOK = 64
CAP = 3
EXPERTS = 64
SLOTS = EXPERTS * CAP
D = 2048
SUB = 16
TOP = 96
F32 = jnp.float32
BF16 = jnp.bfloat16
VMEM = pl.BlockSpec(memory_space=pltpu.VMEM)


def ep_index(z, y, c):
    return (z * Y + y) * C + c


EP_ALL = [(z, y, c) for z in range(Z) for y in range(Y) for c in range(C)]
ROW_OFFSETS = (0, -1, 1, 2)
PLANES = [[ep_index(z, y, c) for z in range(Z)] for y in range(Y) for c in range(C)]


def y_perm(d):
    return [(ep_index(z, y, c), ep_index(z, (y + d) % Y, c)) for z, y, c in EP_ALL]


def core_perm():
    return [(ep_index(z, y, c), ep_index(z, y, 1 - c)) for z, y, c in EP_ALL]


def tp_perm(d):
    return [(i, (i + d) % 4) for i in range(4)]


def cost(flops, nbytes):
    return pl.CostEstimate(flops=flops, bytes_accessed=nbytes, transcendentals=0)


def iota(shape, dim):
    return lax.broadcasted_iota(jnp.int32, shape, dim)


def dot(a, b):
    return jnp.dot(a, b, preferred_element_type=F32)


def swap_matrix():
    out_row, in_row = iota((256, 256), 0), iota((256, 256), 1)
    return jnp.where((out_row // SUB == in_row % SUB) & (out_row % SUB == in_row // SUB), 1.0, 0.0).astype(BF16)


def stack_blocks(rows):
    return jnp.concatenate([rows[:, k * 128 : (k + 1) * 128] for k in range(SUB)], axis=0)


def tile_rows(rows32, out_ref, at):
    both = jnp.concatenate([stack_blocks(rows32[:16]), stack_blocks(rows32[16:])], axis=1)
    tiled = dot(swap_matrix(), both).astype(BF16)
    out_ref[at : at + 256, :] = tiled[:, :128]
    out_ref[at + 256 : at + 512, :] = tiled[:, 128:]


def untile_rows(in_ref, at, out_ref, row):
    both = jnp.concatenate([in_ref[at : at + 256, :], in_ref[at + 256 : at + 512, :]], axis=1)
    y = dot(swap_matrix(), both).astype(BF16)
    for k in range(SUB):
        for i in range(2):
            out_ref[row + i * 16 : row + (i + 1) * 16, k * 128 : (k + 1) * 128] = y[
                k * SUB : (k + 1) * SUB, i * 128 : (i + 1) * 128
            ]


def pair_slots(route_row):
    i0, i1 = iota((128, 128), 0), iota((128, 128), 1)
    wide = jnp.broadcast_to(route_row, (128, 128))
    col = jnp.sum(jnp.where(i0 == i1, wide, 0.0), axis=1, keepdims=True)
    same = (jnp.broadcast_to(col, (128, 128)) == wide) & (i0 < i1)
    rank = jnp.sum(jnp.where(same, 1.0, 0.0), axis=0, keepdims=True)
    return route_row * CAP + rank


def prep_kernel(tp_ref, x_ref, gain_ref, route_ref, out_ref):
    x = x_ref[...].astype(F32)
    scale = lax.rsqrt(jnp.mean(x * x, axis=-1, keepdims=True) + 1e-06)
    normed = (x * scale * gain_ref[...].astype(F32)).astype(BF16)
    slots = pair_slots(route_ref[0].astype(F32))
    chosen = jnp.where(
        iota((SLOTS, 128), 0).astype(F32) == jnp.broadcast_to(slots, (SLOTS, 128)), 1.0, 0.0
    ).astype(BF16)
    owner = jnp.where(iota((128, TOK), 0) // 2 == iota((128, TOK), 1), 1.0, 0.0).astype(BF16)
    select = dot(chosen, owner).astype(BF16)
    sent = dot(select, normed).astype(BF16)
    for b in range(SLOTS // 32):
        tile_rows(sent[b * 32 : (b + 1) * 32], out_ref, b * 512)


def prep(tp, routed_input, gain, routes):
    return pl.pallas_call(
        prep_kernel,
        grid_spec=pltpu.PrefetchScalarGridSpec(
            num_scalar_prefetch=1,
            grid=(1,),
            in_specs=[
                pl.BlockSpec((TOK, D), lambda i, tp: (tp[0], 0)),
                pl.BlockSpec((1, D), lambda i, tp: (0, 0)),
                pl.BlockSpec((1, 1, 128), lambda i, tp: (tp[0], 0, 0)),
            ],
            out_specs=pl.BlockSpec((SLOTS * SUB, 128), lambda i, tp: (0, 0)),
        ),
        out_shape=jax.ShapeDtypeStruct((SLOTS * SUB, 128), BF16),
        cost_estimate=cost(400_000_000, 2_000_000),
        name="prep",
    )(tp, routed_input, gain.reshape(1, D), routes.reshape(4, 1, 128))


def untile_kernel(a_ref, o_ref):
    for b in range(SLOTS // 32):
        untile_rows(a_ref, b * 512, o_ref, b * 32)


def untile(a):
    return pl.pallas_call(
        untile_kernel,
        out_shape=jax.ShapeDtypeStruct((SLOTS, D), BF16),
        in_specs=[VMEM],
        out_specs=VMEM,
        cost_estimate=cost(400_000_000, 1_600_000),
        name="untile",
    )(a)


def expert_rows(x, gate_ref, up_ref, down_ref):
    gate = dot(x, gate_ref[0])
    upper = dot(x, up_ref[0])
    hidden = (gate / (1.0 + jnp.exp(-gate)) * upper).astype(BF16)
    return dot(hidden, down_ref[0]).astype(BF16)


def own_kernel(x_ref, gate_ref, up_ref, down_ref, o_ref):
    o_ref[...] = expert_rows(x_ref[...], gate_ref, up_ref, down_ref)


def own_rows(x, weights):
    return pl.pallas_call(
        own_kernel,
        out_shape=jax.ShapeDtypeStruct((SLOTS, D), BF16),
        in_specs=[VMEM] * 4,
        out_specs=VMEM,
        cost_estimate=cost(600_000_000, 1_600_000),
        name="own_rows",
    )(x, *weights)


def halves_kernel(a_ref, b_ref, gate_ref, up_ref, down_ref, a0_ref, a1_ref, b0_ref, b1_ref):
    for x_ref, lo_ref, hi_ref in ((a_ref, a0_ref, a1_ref), (b_ref, b0_ref, b1_ref)):
        y = expert_rows(x_ref[...], gate_ref, up_ref, down_ref)
        lo_ref[...] = y[:TOP]
        hi_ref[...] = y[TOP:]


def halves(a, b, weights):
    return pl.pallas_call(
        halves_kernel,
        out_shape=[jax.ShapeDtypeStruct((TOP, D), BF16)] * 4,
        in_specs=[VMEM] * 5,
        out_specs=[VMEM] * 4,
        cost_estimate=cost(1_200_000_000, 3_200_000),
        name="halves",
    )(a, b, *weights)


def far_kernel(a_ref, b_ref, gate_ref, up_ref, down_ref, a0_ref, b0_ref):
    y = expert_rows(jnp.concatenate([a_ref[...], b_ref[...]], axis=0), gate_ref, up_ref, down_ref)
    a0_ref[...] = y[:TOP]
    b0_ref[...] = y[TOP:]


def far_rows(a, b, weights):
    return pl.pallas_call(
        far_kernel,
        out_shape=[jax.ShapeDtypeStruct((TOP, D), BF16)] * 2,
        in_specs=[VMEM] * 5,
        out_specs=[VMEM] * 2,
        cost_estimate=cost(600_000_000, 1_600_000),
        name="far_rows",
    )(a, b, *weights)


def add_kernel(a_ref, b_ref, c_ref, d_ref, ab_ref, cd_ref):
    ab_ref[...] = (a_ref[...].astype(F32) + b_ref[...].astype(F32)).astype(BF16)
    cd_ref[...] = (c_ref[...].astype(F32) + d_ref[...].astype(F32)).astype(BF16)


def add_pairs(a, b, c, d):
    return pl.pallas_call(
        add_kernel,
        out_shape=[jax.ShapeDtypeStruct((TOP, D), BF16)] * 2,
        in_specs=[VMEM] * 4,
        out_specs=[VMEM] * 2,
        cost_estimate=cost(10_000_000, 2_400_000),
        name="add_pairs",
    )(a, b, c, d)


def total_kernel(own_ref, a0_ref, b0_ref, a1_ref, b1_ref, o_ref):
    for half, a_ref, b_ref in ((0, a0_ref, b0_ref), (1, a1_ref, b1_ref)):
        for b in range(TOP // 32):
            rows = slice(b * 32, (b + 1) * 32)
            at = half * TOP + b * 32
            added = own_ref[at : at + 32, :].astype(F32) + (
                a_ref[rows, :].astype(F32) + b_ref[rows, :].astype(F32)
            )
            tile_rows(added.astype(BF16), o_ref, at * SUB)


def total(*parts):
    return pl.pallas_call(
        total_kernel,
        out_shape=jax.ShapeDtypeStruct((SLOTS * SUB, 128), BF16),
        in_specs=[VMEM] * 5,
        out_specs=VMEM,
        cost_estimate=cost(400_000_000, 3_000_000),
        name="total",
    )(*parts)


def combine_kernel(tp_ref, r_ref, route_ref, weight_ref, o_ref, plain):
    for b in range(SLOTS // 32):
        untile_rows(r_ref, b * 512, plain, b * 32)
    slots = jnp.broadcast_to(pair_slots(route_ref[0].astype(F32)), (TOK, 128))
    pair, token = iota((TOK, 128), 1), iota((TOK, 128), 0)
    added = None
    for k in range(2):
        col = jnp.sum(jnp.where(pair == 2 * token + k, slots, 0.0), axis=1, keepdims=True)
        pick = jnp.where(
            iota((TOK, SLOTS), 1).astype(F32) == jnp.broadcast_to(col, (TOK, SLOTS)), 1.0, 0.0
        ).astype(BF16)
        term = weight_ref[:, k : k + 1] * dot(pick, plain[...])
        added = term if added is None else added + term
    o_ref[...] = added.astype(BF16)


def combine(tp, back, routes, route_weight):
    return pl.pallas_call(
        combine_kernel,
        grid_spec=pltpu.PrefetchScalarGridSpec(
            num_scalar_prefetch=1,
            grid=(1,),
            in_specs=[
                pl.BlockSpec((SLOTS * SUB, 128), lambda i, tp: (0, 0)),
                pl.BlockSpec((1, 1, 128), lambda i, tp: (tp[0], 0, 0)),
                pl.BlockSpec((TOK, 2), lambda i, tp: (tp[0], 0)),
            ],
            out_specs=pl.BlockSpec((TOK, D), lambda i, tp: (0, 0)),
            scratch_shapes=[pltpu.VMEM((SLOTS, D), BF16)],
        ),
        out_shape=jax.ShapeDtypeStruct((TOK, D), BF16),
        cost_estimate=cost(400_000_000, 2_000_000),
        name="combine",
    )(tp, back, routes.reshape(4, 1, 128), route_weight)


def attend_kernel(ep_ref, q_ref, gate_ref, same_ref, other_ref, o_ref, best, total, summed):
    me = ep_ref[0]
    plane, row, core = me // 8, (me // 2) % 4, me % 2
    q = q_ref[...].astype(F32) * 0.125
    q = jnp.concatenate([q[:, :64], q[:, 64:]], axis=0).astype(BF16)
    own_gate = jnp.broadcast_to(gate_ref[:, pl.ds(pl.multiple_of(me * 128, 128), 128)], (128, 128))
    col = jnp.sum(
        jnp.where(iota((128, 128), 0) == iota((128, 128), 1), own_gate, 0.0), axis=1, keepdims=True
    )
    gate_col = jnp.concatenate([col, col], axis=0)

    def blocks_of(z, low, high):
        return jnp.concatenate(
            [ref[z * 4 + i, low:high, :] for ref in (same_ref, other_ref) for i in range(4)], axis=1
        )

    def starts_of(z):
        return [
            ((z * 4 + (row + dy + 4) % 4) * 2 + c) * 128 for c in (core, 1 - core) for dy in ROW_OFFSETS
        ]

    def scores_of(z):
        gates = [gate_ref[:, pl.ds(pl.multiple_of(at, 128), 128)] for at in starts_of(z)]
        return dot(q, blocks_of(z, 0, 64)) + gate_col - jnp.concatenate(gates, axis=1)

    def weighted(weights, z):
        return lax.dot_general(
            weights.astype(BF16),
            blocks_of(z, 64, 128),
            (((1,), (1,)), ((), ())),
            preferred_element_type=F32,
        )

    scores = scores_of(plane)
    query = iota((256, 128), 0) % 128 + me * 128
    allowed = jnp.concatenate([iota((256, 128), 1) + at <= query for at in starts_of(plane)], axis=1)
    scores = jnp.where(allowed, scores, -jnp.inf)
    top = jnp.max(scores, axis=1, keepdims=True)
    weights = jnp.exp(scores - top)
    best[...] = top
    total[...] = jnp.sum(weights, axis=1, keepdims=True)
    summed[...] = weighted(weights, plane)

    @pl.loop(0, plane)
    def _(z):
        scores = scores_of(z)
        before = best[...]
        top = jnp.maximum(before, jnp.max(scores, axis=1, keepdims=True))
        factor = jnp.exp(before - top)
        weights = jnp.exp(scores - top)
        best[...] = top
        total[...] = total[...] * factor + jnp.sum(weights, axis=1, keepdims=True)
        summed[...] = summed[...] * factor + weighted(weights, z)

    out = summed[...] / total[...]
    o_ref[...] = jnp.concatenate([out[:128], out[128:]], axis=1).astype(BF16)


def attend(ep, queries, cum_gate, same, other):
    return pl.pallas_call(
        attend_kernel,
        out_shape=jax.ShapeDtypeStruct((128, 128), BF16),
        in_specs=[pl.BlockSpec(memory_space=pltpu.SMEM)] + [VMEM] * 4,
        out_specs=VMEM,
        scratch_shapes=[
            pltpu.VMEM((256, 1), F32),
            pltpu.VMEM((256, 1), F32),
            pltpu.VMEM((256, 64), F32),
        ],
        cost_estimate=cost(4_000_000_000, 2_500_000),
        name="attend",
    )(ep, queries, cum_gate, same, other)


def over_experts(x):
    return lax.all_to_all(x.reshape(EXPERTS, 48, 128), "ep", 0, 0, tiled=True).reshape(SLOTS * SUB, 128)


def over_planes(own):
    return lax.all_to_all(
        jnp.broadcast_to(own[None], (Z, 4, 128, 128)),
        "ep",
        0,
        0,
        tiled=True,
        axis_index_groups=PLANES,
    ).reshape(32, 128, 128)


def gather_kv(key_cache, value_cache):
    kv = jnp.concatenate([key_cache[0], value_cache[0]], axis=0)
    own = jnp.stack(
        [kv, lax.ppermute(kv, "ep", y_perm(1)), lax.ppermute(kv, "ep", y_perm(-1)), lax.ppermute(kv, "ep", y_perm(2))]
    )
    same = over_planes(own)
    return same, lax.ppermute(same, "ep", core_perm())


def body(
    queries,
    key_cache,
    value_cache,
    cum_gate,
    out_weight,
    routed_input,
    norm_gain,
    routes,
    route_weight,
    expert_gate,
    expert_up,
    expert_down,
):
    tp = lax.axis_index("tp").astype(jnp.int32).reshape(1)
    ep = lax.axis_index("ep").astype(jnp.int32).reshape(1)
    weights = (expert_gate, expert_up, expert_down)
    came = over_experts(prep(tp, routed_input, norm_gain, routes))
    own = untile(came)
    left = lax.ppermute(own, "tp", tp_perm(1))
    right = lax.ppermute(own, "tp", tp_perm(-1))
    far_top = lax.ppermute(left[:TOP], "tp", tp_perm(1))
    far_bottom = lax.ppermute(right[TOP:], "tp", tp_perm(-1))
    own_part = own_rows(own, weights)
    left_top, left_bottom, right_top, right_bottom = halves(left, right, weights)
    far_top, far_bottom = far_rows(far_top, far_bottom, weights)
    mine_top = lax.ppermute(left_top, "tp", tp_perm(-1))
    mine_bottom = lax.ppermute(right_bottom, "tp", tp_perm(1))
    over_top = lax.ppermute(far_top, "tp", tp_perm(1))
    over_bottom = lax.ppermute(far_bottom, "tp", tp_perm(-1))
    right_top, left_bottom = add_pairs(right_top, over_top, left_bottom, over_bottom)
    also_top = lax.ppermute(right_top, "tp", tp_perm(1))
    also_bottom = lax.ppermute(left_bottom, "tp", tp_perm(-1))
    mine = total(own_part, mine_top, also_top, mine_bottom, also_bottom)
    expert_out = combine(tp, over_experts(mine), routes, route_weight)

    same, other = gather_kv(key_cache, value_cache)
    attended = attend(ep, queries, cum_gate, same, other)
    by_position = lax.all_to_all(attended, "tp", split_axis=0, concat_axis=1, tiled=True)
    mixed_out = jnp.dot(by_position, out_weight, preferred_element_type=F32).astype(BF16)
    return (mixed_out, expert_out)


def solution(mesh):
    return jax.shard_map(
        body,
        mesh=mesh,
        in_specs=(
            P("ep", "tp"),
            P("tp", None, "ep"),
            P("tp", None, "ep"),
            P("tp", None),
            P(),
            P("ep", None),
            P(),
            P("ep", None),
            P("ep", None),
            P("ep", None, "tp"),
            P("ep", None, "tp"),
            P("ep", "tp", None),
        ),
        out_specs=(P(("ep", "tp"), None), P(("ep", "tp"), None)),
        check_vma=False,
    )
```

time: 211 us -> 169 us (0.80)
  blocking collectives: 41.1 us -> 0 us
  starting transfers between devices: 23 us -> 52.1 us
  Pallas kernels: 0 us -> 28.8 us
  matrix products: 22.4 us -> 1.13 us
  between operations: 14.2 us -> 0.83 us
  waiting for transfers between devices: 90 us -> 77.4 us
  other arithmetic: 7.98 us -> 0.03 us
  local copies, waits for them, and re-layouts: 11 us -> 7.71 us
    all_to_all x1 -> x0, blocking collectives: 41.1 us -> none  [expert_half(): lax.all_to_all(outgoing.reshape(1, ep_size, per_device, width), 'ep', spl...]
    pallas_call x0 -> x9, Pallas kernels: none -> 28.8 us  [the longest x1 4.88 us: halves(): pl.pallas_call(halves_kernel, out_shape=[jax.ShapeDtypeStruct((TOP, D), B...]
    dot_general x7 -> x1, matrix products: 22.4 us -> 1.13 us  [body(): jnp.dot(by_position, out_weight, preferred_element_type=F32).astype(BF16)]
    all_gather x1 -> x0, waiting for transfers between devices: 21 us -> none  [side_by_side(): lax.all_gather(both, axis, axis=dim, tiled=True)]
    ppermute x0 -> x14, starting transfers between devices: none -> 18.4 us  [the longest x1 2.68 us: body(): over_bottom = lax.ppermute(far_bottom, 'tp', tp_perm(-1))]
    ppermute x0 -> x14, waiting for transfers between devices: none -> 16.6 us  [the longest x1 8.09 us: body(): far_top = lax.ppermute(left[:TOP], 'tp', tp_perm(1))]
    all_to_all x4, starting transfers between devices: 23 us -> 33.6 us  [the longest x2 26.1 us: over_experts(): lax.all_to_all(x.reshape(EXPERTS, 48, 128), 'ep', 0, 0, tiled=True)]
    all_to_all x4, waiting for transfers between devices: 69 us -> 60.7 us  [the longest x2 36.6 us: over_experts(): lax.all_to_all(x.reshape(EXPERTS, 48, 128), 'ep', 0, 0, tiled=True)]
  transfers between devices with their start and end apart: 5 -> 18, of which waited for: 4 -> 10; matrix products, arithmetic and copies ran while one was open for 12% -> 2% of each run, Pallas kernels for 0% -> 14%
where the time goes in v1:
time: 169 us; the launch traced here: 168 us
  waiting for transfers between devices  77.4 us (46%)
  starting transfers between devices  52.1 us (31%)
  Pallas kernels  28.8 us (17%)
  local copies, waits for them, and re-layouts  7.71 us (5%)
    all_to_all x2, waiting for transfers between devices, over_experts(): lax.all_to_all(x.reshape(EXPERTS, 48, 128), 'ep', 0, 0, tiled=True)  36.6 us
    all_to_all x2, starting transfers between devices, over_experts(): lax.all_to_all(x.reshape(EXPERTS, 48, 128), 'ep', 0, 0, tiled=True)  26.1 us
    all_to_all x1, waiting for transfers between devices, over_planes(): lax.all_to_all(jnp.broadcast_to(own[None], (Z, 4, 128, 128)), 'ep', 0, 0,...  24.1 us
    ppermute x1, waiting for transfers between devices, body(): far_top = lax.ppermute(left[:TOP], 'tp', tp_perm(1))  8.09 us
    pallas_call x1, Pallas kernels, halves(): pl.pallas_call(halves_kernel, out_shape=[jax.ShapeDtypeStruct((TOP, D), B...  4.88 us
    all_to_all x1, starting transfers between devices, over_planes(): lax.all_to_all(jnp.broadcast_to(own[None], (Z, 4, 128, 128)), 'ep', 0, 0,...  4.24 us
    pallas_call x1, Pallas kernels, own_rows(): pl.pallas_call(own_kernel, out_shape=jax.ShapeDtypeStruct((SLOTS, D), BF1...  3.88 us
    pallas_call x1, Pallas kernels, far_rows(): pl.pallas_call(far_kernel, out_shape=[jax.ShapeDtypeStruct((TOP, D), BF16...  3.88 us
  transfers between devices with their start and end apart: 18, of which 10 were waited for; matrix products, arithmetic and copies ran while one was open for 2% of the time, Pallas kernels for 14%

profile of v1, /device:TPU:1, one launch (start us, length us, event | category | flops | bytes accessed | tf_op | source)
XLA Modules:
  0.0 168.0 jit_solution(2072302506611135105)
XLA Ops:
  0.6 0.0 copy-start
  0.7 1.0 copy.22
  1.6 0.7 reshape.40
  2.3 1.3 reshape.39.gain_ref
  3.6 2.7 %prep.1 = bf16[3072,128]{1,0:T(8,128)(2,1)} custom-call(s32[1]{0:T(128)} %bitcast.10.tp_ref, bf16[256,2048]{1,0:T(8,128)(2,1)} %x_ref.1, bf16[1,2048]{1,0:T(2,128)(2,1)} %reshape.39.gain_ref, s32[4,1,128]{2,1,0:T(1,128)} %bitcast.36), custom_call_target="tpu_custom_call" | custom-call | flops 400000000 | bytes 2000000 | tf_op jit(solution)/shard_map/prep/pallas_call | solution.py:106
  6.4 13.1 %all-to-all-start.2 = ((bf16[64,48,128]{2,1,0:T(8,128)(2,1)}), bf16[64,48,128]{2,1,0:T(8,128)(2,1)S(1)}, u32[]{:S(2)}, u32[]{:S(2)}) async-start(bf16[64,48,128]{2,1,0:T(8,128)(2,1)} %bitcast.26), calls=%async_computation.2 | async-start | bytes 1572864 | tf_op jit(solution)/shard_map/all_to_all | solution.py:346
  19.6 1.4 collective-permute-start
  21.0 1.3 collective-permute-start.1
  22.3 1.6 collective-permute-start.2
  24.0 1.0 collective-permute-done
  24.9 0.0 collective-permute-done.1
  24.9 2.0 %collective-permute-done.2 = bf16[128,128]{1,0:T(8,128)(2,1)S(1)} collective-permute-done((bf16[128,128]{1,0:T(8,128)(2,1)S(1)}, bf16[128,128]{1,0:T(8,128)(2,1)S(1)}, u32[]{:S(2)}, u32[]{:S(2)}) %collective-permute-start.2) | collective-permute-done | bytes 32800 | tf_op jit(solution)/shard_map/ppermute | solution.py:363
  27.0 15.5 %all-to-all-done.2 = bf16[64,48,128]{2,1,0:T(8,128)(2,1)S(1)} async-done(((bf16[64,48,128]{2,1,0:T(8,128)(2,1)}), bf16[64,48,128]{2,1,0:T(8,128)(2,1)S(1)}, u32[]{:S(2)}, u32[]{:S(2)}) %all-to-all-start.2) | async-done | bytes 786464 | tf_op jit(solution)/shard_map/all_to_all | solution.py:346
  42.5 1.2 broadcast_in_dim.2
  43.8 4.2 %all-to-all-start = ((bf16[8,4,128,128]{3,2,1,0:T(8,128)(2,1)}), bf16[8,4,128,128]{3,2,1,0:T(8,128)(2,1)}, u32[]{:S(2)}, u32[]{:S(2)}) async-start(bf16[8,4,128,128]{3,2,1,0:T(8,128)(2,1)} %broadcast_in_dim.2), calls=%async_computation | async-start | bytes 2097152 | tf_op jit(solution)/shard_map/all_to_all | solution.py:350
  48.0 2.4 %untile.1.x_ref = bf16[192,2048]{1,0:T(8,128)(2,1)} custom-call(bf16[3072,128]{1,0:T(8,128)(2,1)} %bitcast.27), custom_call_target="tpu_custom_call" | custom-call | flops 400000000 | bytes 1600000 | tf_op jit(solution)/shard_map/untile/pallas_call | solution.py:130
  50.4 1.2 collective-permute-start.4
  51.7 1.5 collective-permute-start.5
  53.1 24.1 %all-to-all-done = bf16[8,4,128,128]{3,2,1,0:T(8,128)(2,1)} async-done(((bf16[8,4,128,128]{3,2,1,0:T(8,128)(2,1)}), bf16[8,4,128,128]{3,2,1,0:T(8,128)(2,1)}, u32[]{:S(2)}, u32[]{:S(2)}) %all-to-all-start) | async-done | bytes 1048608 | tf_op jit(solution)/shard_map/all_to_all | solution.py:350
  77.2 0.5 collective-permute-start.3
  77.8 1.3 collective-permute-start.7
  79.1 0.0 collective-permute-done.5.b_ref
  79.1 1.0 slice.9
  80.1 1.5 collective-permute-start.8
  81.6 8.1 %collective-permute-done.7.a_ref = bf16[96,2048]{1,0:T(8,128)(2,1)S(1)} collective-permute-done((bf16[96,2048]{1,0:T(8,128)(2,1)S(1)}, bf16[96,2048]{1,0:T(8,128)(2,1)S(1)}, u32[]{:S(2)}, u32[]{:S(2)}) %collective-permute-start.7) | collective-permute-done | bytes 393248 | tf_op jit(solution)/shard_map/ppermute | solution.py:390
  89.7 0.9 collective-permute-done.8.b_ref
  90.7 3.9 %far_rows.1 = (bf16[96,2048]{1,0:T(8,128)(2,1)}, bf16[96,2048]{1,0:T(8,128)(2,1)}) custom-call(bf16[96,2048]{1,0:T(8,128)(2,1)} %copy-done.8, bf16[96,2048]{1,0:T(8,128)(2,1)} %collective-permute-done.8.b_ref, bf16[1,2048,256]{2,1,0:T(8,128)(2,1)} %gate_ref.7, bf16[1,2048,256]{2,1,0:T(8,128)(2,1)} %up_ref.5, bf16[1,256,2048]{2,1,0:T(8,128)(2,1)} %down_ref.5), custom_call_target="tpu_custom_call" | custom-call | flops 600000000 | bytes 1600000 | tf_op jit(solution)/shard_map/far_rows/pallas_call | solution.py:187
  94.5 2.7 %collective-permute-start.10 = (bf16[96,2048]{1,0:T(8,128)(2,1)}, bf16[96,2048]{1,0:T(8,128)(2,1)S(1)}, u32[]{:S(2)}, u32[]{:S(2)}) collective-permute-start(bf16[96,2048]{1,0:T(8,128)(2,1)} %get-tuple-element.14), channel_id=1, source_target_pairs={{0,3},{1,0},{2,1},{3,2},{4,7},{5,4},{6,5},{7,6},{8,11},{9,8},{10,9... | collective-permute-start | bytes 1179656 | tf_op jit(solution)/shard_map/ppermute | solution.py:398
  97.2 4.9 %halves.1 = (bf16[96,2048]{1,0:T(8,128)(2,1)}, bf16[96,2048]{1,0:T(8,128)(2,1)}, bf16[96,2048]{1,0:T(8,128)(2,1)}, bf16[96,2048]{1,0:T(8,128)(2,1)}) custom-call(bf16[192,2048]{1,0:T(8,128)(2,1)} %copy-done.2, bf16[192,2048]{1,0:T(8,128)(2,1)} %collective-permute-done.5.b_ref, bf16[1,2048,256]{2,1,0:T(8,128)(2,1)} %gate_ref.7, bf16[1,2048,256]{2,1,0:T(8,128)(2,1)} %up_ref.5, ...), custom_call_target="tpu_custom_call" | custom-call | flops 1200000000 | bytes 3200000 | tf_op jit(solution)/shard_map/halves/pallas_call | solution.py:170
  102.1 0.0 collective-permute-start.12
  102.1 2.7 %collective-permute-start.6 = (bf16[96,2048]{1,0:T(8,128)(2,1)}, bf16[96,2048]{1,0:T(8,128)(2,1)S(1)}, u32[]{:S(2)}, u32[]{:S(2)}) collective-permute-start(bf16[96,2048]{1,0:T(8,128)(2,1)} %get-tuple-element.10), channel_id=1, source_target_pairs={{0,3},{1,0},{2,1},{3,2},{4,7},{5,4},{6,5},{7,6},{8,11},{9,8},{10,9... | collective-permute-start | bytes 1179656 | tf_op jit(solution)/shard_map/ppermute | solution.py:395
  104.8 0.1 collective-permute-done.10.d_ref
  104.9 3.1 %collective-permute-done.9.b_ref = bf16[96,2048]{1,0:T(8,128)(2,1)} collective-permute-done((bf16[96,2048]{1,0:T(8,128)(2,1)}, bf16[96,2048]{1,0:T(8,128)(2,1)}, u32[]{:S(2)}, u32[]{:S(2)}) %collective-permute-start.9) | collective-permute-done | bytes 393248 | tf_op jit(solution)/shard_map/ppermute | solution.py:397
  108.0 2.3 %add_pairs.1 = (bf16[96,2048]{1,0:T(8,128)(2,1)}, bf16[96,2048]{1,0:T(8,128)(2,1)}) custom-call(bf16[96,2048]{1,0:T(8,128)(2,1)} %get-tuple-element.11.a_ref, bf16[96,2048]{1,0:T(8,128)(2,1)} %collective-permute-done.9.b_ref, bf16[96,2048]{1,0:T(8,128)(2,1)} %get-tuple-element.13.c_ref, bf16[96,2048]{1,0:T(8,128)(2,1)} %copy-done.7), custom_call_target="tpu_custom_call" | custom-call | flops 10000000 | bytes 2400000 | tf_op jit(solution)/shard_map/add_pairs/pallas_call | solution.py:203
  110.3 2.7 %collective-permute-start.13 = (bf16[96,2048]{1,0:T(8,128)(2,1)}, bf16[96,2048]{1,0:T(8,128)(2,1)}, u32[]{:S(2)}, u32[]{:S(2)}) collective-permute-start(bf16[96,2048]{1,0:T(8,128)(2,1)} %get-tuple-element.17), channel_id=1, source_target_pairs={{0,3},{1,0},{2,1},{3,2},{4,7},{5,4},{6,5},{7,6},{8,11},{9,8},{10,9... | collective-permute-start | bytes 1179656 | tf_op jit(solution)/shard_map/ppermute | solution.py:401
  113.0 3.9 %own_rows.1.own_ref = bf16[192,2048]{1,0:T(8,128)(2,1)} custom-call(bf16[192,2048]{1,0:T(8,128)(2,1)} %untile.1.x_ref, bf16[1,2048,256]{2,1,0:T(8,128)(2,1)} %gate_ref.7, bf16[1,2048,256]{2,1,0:T(8,128)(2,1)} %up_ref.5, bf16[1,256,2048]{2,1,0:T(8,128)(2,1)} %down_ref.5), custom_call_target="tpu_custom_call" | custom-call | flops 600000000 | bytes 1600000 | tf_op jit(solution)/shard_map/own_rows/pallas_call | solution.py:152
  116.9 3.2 %attend.1 = bf16[128,128]{1,0:T(8,128)(2,1)} custom-call(s32[1]{0:T(128)} %bitcast.ep_ref, bf16[128,128]{1,0:T(8,128)(2,1)} %q_ref.1, f32[1,8192]{1,0:T(1,128)} %gate_ref.4, bf16[32,128,128]{2,1,0:T(8,128)(2,1)} %bitcast.7.same_ref, bf16[32,128,128]{2,1,0:T(8,128)(2,1)} %collective-permute-done.3.other_ref), custom_call_target="tpu_custom_call" | custom-call | flops 4000000000 | bytes 2500000 | tf_op jit(solution)/shard_map/attend/pallas_call | solution.py:330
  120.0 3.3 %all-to-all-start.1 = ((bf16[4,32,128]{2,1,0:T(8,128)(2,1)}), bf16[4,32,128]{2,1,0:T(8,128)(2,1)S(1)}, u32[]{:S(2)}, u32[]{:S(2)}) async-start(bf16[4,32,128]{2,1,0:T(8,128)(2,1)} %bitcast.30), calls=%async_computation.1 | async-start | bytes 65536 | tf_op jit(solution)/shard_map/all_to_all | solution.py:407
  123.3 0.0 copy-start.11
  123.4 1.4 collective-permute-done.11.b0_ref
  124.8 0.7 copy-done.6
  125.5 3.0 %total.1 = bf16[3072,128]{1,0:T(8,128)(2,1)} custom-call(bf16[192,2048]{1,0:T(8,128)(2,1)} %own_rows.1.own_ref, bf16[96,2048]{1,0:T(8,128)(2,1)} %copy-done.5, bf16[96,2048]{1,0:T(8,128)(2,1)} %copy-done.6, bf16[96,2048]{1,0:T(8,128)(2,1)} %copy-done.4, bf16[96,2048]{1,0:T(8,128)(2,1)} %collective-permute-done.13.b1_ref), custom_call_target="tpu_custom_call" | custom-call | flops 400000000 | bytes 3000000 | tf_op jit(solution)/shard_map/total/pallas_call | solution.py:225
  128.5 13.0 %all-to-all-start.3 = ((bf16[64,48,128]{2,1,0:T(8,128)(2,1)}), bf16[64,48,128]{2,1,0:T(8,128)(2,1)S(1)}, u32[]{:S(2)}, u32[]{:S(2)}) async-start(bf16[64,48,128]{2,1,0:T(8,128)(2,1)} %bitcast.28), calls=%async_computation.3 | async-start | bytes 1572864 | tf_op jit(solution)/shard_map/all_to_all | solution.py:346
  141.5 0.8 copy.25.weight_ref
  142.3 1.1 convolution_convert_fusion
  143.5 21.1 %all-to-all-done.3 = bf16[64,48,128]{2,1,0:T(8,128)(2,1)S(1)} async-done(((bf16[64,48,128]{2,1,0:T(8,128)(2,1)}), bf16[64,48,128]{2,1,0:T(8,128)(2,1)S(1)}, u32[]{:S(2)}, u32[]{:S(2)}) %all-to-all-start.3) | async-done | bytes 786464 | tf_op jit(solution)/shard_map/all_to_all | solution.py:346
  164.5 0.9 copy-done.3
  165.4 2.5 %combine.1 = bf16[64,2048]{1,0:T(8,128)(2,1)} custom-call(s32[1]{0:T(128)} %bitcast.10.tp_ref, bf16[3072,128]{1,0:T(8,128)(2,1)} %bitcast.29, s32[4,1,128]{2,1,0:T(1,128)} %bitcast.37, f32[256,2]{1,0:T(8,128)} %copy.25.weight_ref), custom_call_target="tpu_custom_call" | custom-call | flops 400000000 | bytes 2000000 | tf_op jit(solution)/shard_map/combine/pallas_call | solution.py:252
  (31 shorter events, 0.1 us)
Async XLA Ops:
  0.6 141.7 %copy-start = (bf16[512,2048]{1,0:T(8,128)(2,1)S(1)}, bf16[512,2048]{1,0:T(8,128)(2,1)}, u32[]{:S(2)}) copy-start(bf16[512,2048]{1,0:T(8,128)(2,1)} %param.16) | copy-start | bytes 6291460
  0.6 18.9 %copy-start.10 = (bf16[1,64,128]{2,1,0:T(8,128)(2,1)S(1)}, bf16[1,64,128]{2,1,0:T(8,128)(2,1)}, u32[]{:S(2)}) copy-start(bf16[1,64,128]{2,1,0:T(8,128)(2,1)} %param.13) | copy-start | bytes 49156
  0.7 18.9 %copy-start.9 = (bf16[1,64,128]{2,1,0:T(8,128)(2,1)S(1)}, bf16[1,64,128]{2,1,0:T(8,128)(2,1)}, u32[]{:S(2)}) copy-start(bf16[1,64,128]{2,1,0:T(8,128)(2,1)} %param.14) | copy-start | bytes 49156
  6.4 36.2 %all-to-all-start.2 = ((bf16[64,48,128]{2,1,0:T(8,128)(2,1)}), bf16[64,48,128]{2,1,0:T(8,128)(2,1)S(1)}, u32[]{:S(2)}, u32[]{:S(2)}) async-start(bf16[64,48,128]{2,1,0:T(8,128)(2,1)} %bitcast.26), calls=%async_computation.2 | async-start | bytes 1572864 | tf_op jit(solution)/shard_map/all_to_all | solution.py:346
  19.6 5.4 %collective-permute-start = (bf16[128,128]{1,0:T(8,128)(2,1)S(1)}, bf16[128,128]{1,0:T(8,128)(2,1)S(1)}, u32[]{:S(2)}, u32[]{:S(2)}) collective-permute-start(bf16[128,128]{1,0:T(8,128)(2,1)S(1)} %get-tuple-element.19), channel_id=1, source_target_pairs={{0,8},{4,12},{8,16},{12,20},{16,24},{20,28},{24,0},{28,4},{32,40},... | collective-permute-start | bytes 98312 | tf_op jit(solution)/shard_map/ppermute | solution.py:363
  21.0 4.0 %collective-permute-start.1 = (bf16[128,128]{1,0:T(8,128)(2,1)S(1)}, bf16[128,128]{1,0:T(8,128)(2,1)S(1)}, u32[]{:S(2)}, u32[]{:S(2)}) collective-permute-start(bf16[128,128]{1,0:T(8,128)(2,1)S(1)} %get-tuple-element.19), channel_id=1, source_target_pairs={{0,24},{4,28},{8,0},{12,4},{16,8},{20,12},{24,16},{28,20},{32,56},... | collective-permute-start | bytes 98312 | tf_op jit(solution)/shard_map/ppermute | solution.py:363
  22.3 4.6 %collective-permute-start.2 = (bf16[128,128]{1,0:T(8,128)(2,1)S(1)}, bf16[128,128]{1,0:T(8,128)(2,1)S(1)}, u32[]{:S(2)}, u32[]{:S(2)}) collective-permute-start(bf16[128,128]{1,0:T(8,128)(2,1)S(1)} %get-tuple-element.19), channel_id=1, source_target_pairs={{0,16},{4,20},{8,24},{12,28},{16,0},{20,4},{24,8},{28,12},{32,48},... | collective-permute-start | bytes 98312 | tf_op jit(solution)/shard_map/ppermute | solution.py:363
  42.5 5.5 %copy-start.1 = (bf16[64,48,128]{2,1,0:T(8,128)(2,1)}, bf16[64,48,128]{2,1,0:T(8,128)(2,1)S(1)}, u32[]{:S(2)}) copy-start(bf16[64,48,128]{2,1,0:T(8,128)(2,1)S(1)} %all-to-all-done.2) | copy-start | bytes 2359300
  43.8 33.5 %all-to-all-start = ((bf16[8,4,128,128]{3,2,1,0:T(8,128)(2,1)}), bf16[8,4,128,128]{3,2,1,0:T(8,128)(2,1)}, u32[]{:S(2)}, u32[]{:S(2)}) async-start(bf16[8,4,128,128]{3,2,1,0:T(8,128)(2,1)} %broadcast_in_dim.2), calls=%async_computation | async-start | bytes 2097152 | tf_op jit(solution)/shard_map/all_to_all | solution.py:350
  50.4 27.3 %collective-permute-start.4 = (bf16[192,2048]{1,0:T(8,128)(2,1)}, bf16[192,2048]{1,0:T(8,128)(2,1)S(1)}, u32[]{:S(2)}, u32[]{:S(2)}) collective-permute-start(bf16[192,2048]{1,0:T(8,128)(2,1)} %untile.1.x_ref), channel_id=1, source_target_pairs={{0,1},{1,2},{2,3},{3,0},{4,5},{5,6},{6,7},{7,4},{8,9},{9,10},{10,1... | collective-permute-start | bytes 2359304 | tf_op jit(solution)/shard_map/ppermute | solution.py:388
  51.7 27.4 %collective-permute-start.5 = (bf16[192,2048]{1,0:T(8,128)(2,1)}, bf16[192,2048]{1,0:T(8,128)(2,1)}, u32[]{:S(2)}, u32[]{:S(2)}) collective-permute-start(bf16[192,2048]{1,0:T(8,128)(2,1)} %untile.1.x_ref), channel_id=1, source_target_pairs={{0,3},{1,0},{2,1},{3,2},{4,7},{5,4},{6,5},{7,6},{8,11},{9,8},{10,9... | collective-permute-start | bytes 2359304 | tf_op jit(solution)/shard_map/ppermute | solution.py:389
  77.2 39.6 %collective-permute-start.3 = (bf16[32,128,128]{2,1,0:T(8,128)(2,1)}, bf16[32,128,128]{2,1,0:T(8,128)(2,1)}, u32[]{:S(2)}, u32[]{:S(2)}) collective-permute-start(bf16[32,128,128]{2,1,0:T(8,128)(2,1)} %bitcast.7.same_ref), channel_id=1, source_target_pairs={{0,4},{4,0},{8,12},{12,8},{16,20},{20,16},{24,28},{28,24},{32,36},... | collective-permute-start | bytes 3145736 | tf_op jit(solution)/shard_map/ppermute | solution.py:366
  77.7 16.8 %copy-start.2 = (bf16[192,2048]{1,0:T(8,128)(2,1)}, bf16[192,2048]{1,0:T(8,128)(2,1)S(1)}, u32[]{:S(2)}) copy-start(bf16[192,2048]{1,0:T(8,128)(2,1)S(1)} %collective-permute-done.4.a_ref) | copy-start | bytes 2359300
  77.8 11.9 %collective-permute-start.7 = (bf16[96,2048]{1,0:T(8,128)(2,1)S(1)}, bf16[96,2048]{1,0:T(8,128)(2,1)S(1)}, u32[]{:S(2)}, u32[]{:S(2)}) collective-permute-start(bf16[96,2048]{1,0:T(8,128)(2,1)S(1)} %slice.8), channel_id=1, source_target_pairs={{0,1},{1,2},{2,3},{3,0},{4,5},{5,6},{6,7},{7,4},{8,9},{9,10},{10,1... | collective-permute-start | bytes 1179656 | tf_op jit(solution)/shard_map/ppermute | solution.py:390
  80.1 10.6 %collective-permute-start.8 = (bf16[96,2048]{1,0:T(8,128)(2,1)S(1)}, bf16[96,2048]{1,0:T(8,128)(2,1)}, u32[]{:S(2)}, u32[]{:S(2)}) collective-permute-start(bf16[96,2048]{1,0:T(8,128)(2,1)S(1)} %slice.9), channel_id=1, source_target_pairs={{0,3},{1,0},{2,1},{3,2},{4,7},{5,4},{6,5},{7,6},{8,11},{9,8},{10,9... | collective-permute-start | bytes 1179656 | tf_op jit(solution)/shard_map/ppermute | solution.py:391
  89.7 0.9 copy-start.8
  94.5 10.3 %collective-permute-start.10 = (bf16[96,2048]{1,0:T(8,128)(2,1)}, bf16[96,2048]{1,0:T(8,128)(2,1)S(1)}, u32[]{:S(2)}, u32[]{:S(2)}) collective-permute-start(bf16[96,2048]{1,0:T(8,128)(2,1)} %get-tuple-element.14), channel_id=1, source_target_pairs={{0,3},{1,0},{2,1},{3,2},{4,7},{5,4},{6,5},{7,6},{8,11},{9,8},{10,9... | collective-permute-start | bytes 1179656 | tf_op jit(solution)/shard_map/ppermute | solution.py:398
  97.2 10.8 %collective-permute-start.9 = (bf16[96,2048]{1,0:T(8,128)(2,1)}, bf16[96,2048]{1,0:T(8,128)(2,1)}, u32[]{:S(2)}, u32[]{:S(2)}) collective-permute-start(bf16[96,2048]{1,0:T(8,128)(2,1)} %get-tuple-element.12), channel_id=1, source_target_pairs={{0,1},{1,2},{2,3},{3,0},{4,5},{5,6},{6,7},{7,4},{8,9},{9,10},{10,1... | collective-permute-start | bytes 1179656 | tf_op jit(solution)/shard_map/ppermute | solution.py:397
  102.1 21.2 %collective-permute-start.12 = (bf16[96,2048]{1,0:T(8,128)(2,1)}, bf16[96,2048]{1,0:T(8,128)(2,1)S(1)}, u32[]{:S(2)}, u32[]{:S(2)}) collective-permute-start(bf16[96,2048]{1,0:T(8,128)(2,1)} %get-tuple-element.16), channel_id=1, source_target_pairs={{0,1},{1,2},{2,3},{3,0},{4,5},{5,6},{6,7},{7,4},{8,9},{9,10},{10,1... | collective-permute-start | bytes 1179656 | tf_op jit(solution)/shard_map/ppermute | solution.py:396
  102.1 21.2 %collective-permute-start.6 = (bf16[96,2048]{1,0:T(8,128)(2,1)}, bf16[96,2048]{1,0:T(8,128)(2,1)S(1)}, u32[]{:S(2)}, u32[]{:S(2)}) collective-permute-start(bf16[96,2048]{1,0:T(8,128)(2,1)} %get-tuple-element.10), channel_id=1, source_target_pairs={{0,3},{1,0},{2,1},{3,2},{4,7},{5,4},{6,5},{7,6},{8,11},{9,8},{10,9... | collective-permute-start | bytes 1179656 | tf_op jit(solution)/shard_map/ppermute | solution.py:395
  104.9 3.1 %copy-start.7 = (bf16[96,2048]{1,0:T(8,128)(2,1)}, bf16[96,2048]{1,0:T(8,128)(2,1)S(1)}, u32[]{:S(2)}) copy-start(bf16[96,2048]{1,0:T(8,128)(2,1)S(1)} %collective-permute-done.10.d_ref) | copy-start | bytes 1179652
  110.3 14.4 %collective-permute-start.11 = (bf16[96,2048]{1,0:T(8,128)(2,1)}, bf16[96,2048]{1,0:T(8,128)(2,1)S(1)}, u32[]{:S(2)}, u32[]{:S(2)}) collective-permute-start(bf16[96,2048]{1,0:T(8,128)(2,1)} %get-tuple-element.15), channel_id=1, source_target_pairs={{0,1},{1,2},{2,3},{3,0},{4,5},{5,6},{6,7},{7,4},{8,9},{9,10},{10,1... | collective-permute-start | bytes 1179656 | tf_op jit(solution)/shard_map/ppermute | solution.py:400
  110.3 14.4 %collective-permute-start.13 = (bf16[96,2048]{1,0:T(8,128)(2,1)}, bf16[96,2048]{1,0:T(8,128)(2,1)}, u32[]{:S(2)}, u32[]{:S(2)}) collective-permute-start(bf16[96,2048]{1,0:T(8,128)(2,1)} %get-tuple-element.17), channel_id=1, source_target_pairs={{0,3},{1,0},{2,1},{3,2},{4,7},{5,4},{6,5},{7,6},{8,11},{9,8},{10,9... | collective-permute-start | bytes 1179656 | tf_op jit(solution)/shard_map/ppermute | solution.py:401
  120.0 8.5 %all-to-all-start.1 = ((bf16[4,32,128]{2,1,0:T(8,128)(2,1)}), bf16[4,32,128]{2,1,0:T(8,128)(2,1)S(1)}, u32[]{:S(2)}, u32[]{:S(2)}) async-start(bf16[4,32,128]{2,1,0:T(8,128)(2,1)} %bitcast.30), calls=%async_computation.1 | async-start | bytes 65536 | tf_op jit(solution)/shard_map/all_to_all | solution.py:407
  123.3 18.2 %copy-start.11 = (f32[256,2]{0,1:T(2,128)S(1)}, f32[256,2]{0,1:T(2,128)}, u32[]{:S(2)}) copy-start(f32[256,2]{0,1:T(2,128)} %param.20) | copy-start | bytes 6148
  123.3 1.4 copy-start.4
  123.3 1.4 copy-start.5
  124.7 0.8 copy-start.6
  128.5 36.0 %all-to-all-start.3 = ((bf16[64,48,128]{2,1,0:T(8,128)(2,1)}), bf16[64,48,128]{2,1,0:T(8,128)(2,1)S(1)}, u32[]{:S(2)}, u32[]{:S(2)}) async-start(bf16[64,48,128]{2,1,0:T(8,128)(2,1)} %bitcast.28), calls=%async_computation.3 | async-start | bytes 1572864 | tf_op jit(solution)/shard_map/all_to_all | solution.py:346
  164.5 0.9 copy-start.3

commit v2 on v1

v2 whole, which is shorter than its diff:
```python
import functools

import jax
import jax.numpy as jnp
from jax import lax
from jax.experimental import pallas as pl
from jax.experimental.pallas import tpu as pltpu
from jax.sharding import PartitionSpec as P


Z, Y, C = 8, 4, 2
TOK = 64
CAP = 3
EXPERTS = 64
SLOTS = EXPERTS * CAP
D = 2048
SUB = 16
TOP = 96
F32 = jnp.float32
BF16 = jnp.bfloat16
VMEM = pl.BlockSpec(memory_space=pltpu.VMEM)
SMEM = pl.BlockSpec(memory_space=pltpu.SMEM)
HBM = pl.BlockSpec(memory_space=pltpu.HBM)
LIMIT = pltpu.CompilerParams(vmem_limit_bytes=12 * 1024 * 1024)


def ep_index(z, y, c):
    return (z * Y + y) * C + c


EP_ALL = [(z, y, c) for z in range(Z) for y in range(Y) for c in range(C)]
ROW_OFFSETS = (0, -1, 1, 2)
TP_SHIFTS = (0, 1, -1, 2)
PLANES = [[ep_index(z, y, c) for z in range(Z)] for y in range(Y) for c in range(C)]


def y_perm(d):
    return [(ep_index(z, y, c), ep_index(z, (y + d) % Y, c)) for z, y, c in EP_ALL]


def core_perm():
    return [(ep_index(z, y, c), ep_index(z, y, 1 - c)) for z, y, c in EP_ALL]


def tp_perm(d):
    return [(i, (i + d) % 4) for i in range(4)]


def cost(flops, nbytes):
    return pl.CostEstimate(flops=flops, bytes_accessed=nbytes, transcendentals=0)


def near(x):
    return pltpu.with_memory_space_constraint(x, pltpu.VMEM)


def near_out(shape, dtype=BF16):
    return pltpu.VMEM(shape, dtype)


def iota(shape, dim):
    return lax.broadcasted_iota(jnp.int32, shape, dim)


def dot(a, b):
    return jnp.dot(a, b, preferred_element_type=F32)


def swap_matrix():
    out_row, in_row = iota((256, 256), 0), iota((256, 256), 1)
    return jnp.where((out_row // SUB == in_row % SUB) & (out_row % SUB == in_row // SUB), 1.0, 0.0).astype(BF16)


def stack_blocks(rows):
    return jnp.concatenate([rows[:, k * 128 : (k + 1) * 128] for k in range(SUB)], axis=0)


def tile_rows(rows, scratch, out_hbm, sems):
    copies = []
    for part in range(3):
        groups = range(part * 4, part * 4 + 4)
        wide = jnp.concatenate([stack_blocks(rows[g * 16 : (g + 1) * 16]) for g in groups], axis=1)
        tiled = dot(swap_matrix(), wide).astype(BF16)
        for i, g in enumerate(groups):
            scratch[g * 256 : (g + 1) * 256, :] = tiled[:, i * 128 : (i + 1) * 128]
        here = pl.ds(part * 1024, 1024)
        copies.append(pltpu.make_async_copy(scratch.at[here, :], out_hbm.at[here, :], sems.at[part]))
        copies[-1].start()
    for copy in copies:
        copy.wait()


def untile_groups(in_ref, groups, place):
    wide = jnp.concatenate([in_ref[g * 256 : (g + 1) * 256, :] for g in groups], axis=1)
    y = dot(swap_matrix(), wide).astype(BF16)
    for i, g in enumerate(groups):
        ref, row = place(g)
        for k in range(SUB):
            ref[row : row + 16, k * 128 : (k + 1) * 128] = y[k * SUB : (k + 1) * SUB, i * 128 : (i + 1) * 128]


TILES = [pltpu.VMEM((SLOTS * SUB, 128), BF16), pltpu.SemaphoreType.DMA((3,))]


def own_lanes(ref, tp):
    whole = ref[...].astype(F32)
    return sum(jnp.where(tp == j, whole[:, j * TOK : (j + 1) * TOK], 0.0) for j in range(4))


def column(row):
    n = row.shape[1]
    wide = jnp.broadcast_to(row, (n, n))
    return jnp.sum(jnp.where(iota((n, n), 0) == iota((n, n), 1), wide, 0.0), axis=1, keepdims=True)


def pair_slots(route_ref, tp):
    routes = own_lanes(route_ref, tp)
    row = jnp.concatenate([routes[0:1], routes[1:2]], axis=1)
    wide = jnp.broadcast_to(row, (128, 128))
    same = jnp.broadcast_to(column(row), (128, 128)) == wide
    earlier = iota((128, 128), 0) % TOK < iota((128, 128), 1) % TOK
    rank = jnp.sum(jnp.where(same & earlier, 1.0, 0.0), axis=0, keepdims=True)
    return row * CAP + rank


def prep_kernel(tp_ref, x_hbm, gain_hbm, route_hbm, out_hbm, x_ref, gain_ref, route_ref, loaded, scratch, sems):
    tp = tp_ref[0]
    mine = x_hbm.at[pl.ds(pl.multiple_of(tp * TOK, TOK), TOK), :]
    pairs = ((route_hbm, route_ref), (mine, x_ref), (gain_hbm, gain_ref))
    copies = [pltpu.make_async_copy(here, there, loaded.at[i]) for i, (here, there) in enumerate(pairs)]
    for copy in copies:
        copy.start()
    copies[0].wait()
    slots = jnp.broadcast_to(pair_slots(route_ref, tp), (SLOTS, 128))
    chosen = jnp.where(iota((SLOTS, 128), 0).astype(F32) == slots, 1.0, 0.0)
    select = (chosen[:, :TOK] + chosen[:, TOK:]).astype(BF16)
    copies[1].wait()
    copies[2].wait()
    x = x_ref[...].astype(F32)
    scale = lax.rsqrt(jnp.mean(x * x, axis=-1, keepdims=True) + 1e-06)
    normed = (x * scale * gain_ref[...].astype(F32).reshape(1, D)).astype(BF16)
    tile_rows(dot(select, normed).astype(BF16), scratch, out_hbm, sems)


def prep(tp, routed_input, gain, routes):
    return pl.pallas_call(
        prep_kernel,
        in_specs=[SMEM, HBM, HBM, HBM],
        out_specs=HBM,
        out_shape=pltpu.HBM((SLOTS * SUB, 128), BF16),
        scratch_shapes=[
            pltpu.VMEM((TOK, D), BF16),
            pltpu.VMEM((D,), BF16),
            pltpu.VMEM((2, 4 * TOK), jnp.int32),
            pltpu.SemaphoreType.DMA((3,)),
        ]
        + TILES,
        cost_estimate=cost(400_000_000, 2_000_000),
        name="prep",
        compiler_params=LIMIT,
    )(tp, *(pltpu.with_memory_space_constraint(x, pltpu.HBM) for x in (routed_input, gain, routes.T)))


def untile_kernel(a_hbm, top_ref, bottom_ref, scratch, sems):
    copies = []
    for part in range(3):
        here = pl.ds(part * 1024, 1024)
        copies.append(pltpu.make_async_copy(a_hbm.at[here, :], scratch.at[here, :], sems.at[part]))
        copies[-1].start()
    for part in range(3):
        copies[part].wait()
        untile_groups(
            scratch,
            range(part * 4, part * 4 + 4),
            lambda g: (top_ref, g * 16) if g < TOP // 16 else (bottom_ref, g * 16 - TOP),
        )


def untile(a):
    return pl.pallas_call(
        untile_kernel,
        out_shape=[near_out((TOP, D))] * 2,
        in_specs=[HBM],
        out_specs=[VMEM] * 2,
        scratch_shapes=TILES,
        cost_estimate=cost(400_000_000, 1_600_000),
        name="untile",
        compiler_params=LIMIT,
    )(pltpu.with_memory_space_constraint(a, pltpu.HBM))


def rows_kernel(count, *refs):
    blocks, (gate_ref, up_ref, down_ref), outs = refs[: -count - 3], refs[-count - 3 : -count], refs[-count:]
    x = jnp.concatenate([ref[...] for ref in blocks], axis=0)
    gate = dot(x, gate_ref[0])
    upper = dot(x, up_ref[0])
    hidden = (gate / (1.0 + jnp.exp(-gate)) * upper).astype(BF16)
    result = dot(hidden, down_ref[0]).astype(BF16)
    rows = result.shape[0] // count
    for i, out in enumerate(outs):
        out[...] = result[i * rows : (i + 1) * rows]


def expert_rows(weights, places, *blocks):
    rows = sum(b.shape[0] for b in blocks)
    count = len(places)
    return pl.pallas_call(
        functools.partial(rows_kernel, count),
        out_shape=[place((rows // count, D), BF16) for place in places],
        in_specs=[VMEM] * (len(blocks) + 3),
        out_specs=[VMEM] * count,
        cost_estimate=cost(3_000_000 * rows, 8_000 * rows),
        name="expert_rows",
        compiler_params=LIMIT,
    )(*(near(b) for b in blocks), *weights)


def add_kernel(a_ref, b_ref, c_ref, d_ref, ab_ref, cd_ref):
    ab_ref[...] = (a_ref[...].astype(F32) + b_ref[...].astype(F32)).astype(BF16)
    cd_ref[...] = (c_ref[...].astype(F32) + d_ref[...].astype(F32)).astype(BF16)


def add_pairs(kept_a, came_a, kept_b, came_b):
    return pl.pallas_call(
        add_kernel,
        out_shape=[near_out((TOP, D))] * 2,
        in_specs=[VMEM] * 4,
        out_specs=[VMEM] * 2,
        cost_estimate=cost(10_000_000, 2_400_000),
        name="add_pairs",
        compiler_params=LIMIT,
    )(kept_a, near(came_a), kept_b, near(came_b))


def total_kernel(own_ref, a0_ref, b0_ref, a1_ref, b1_ref, out_hbm, scratch, sems):
    added = [
        own_ref[i * TOP : (i + 1) * TOP, :].astype(F32) + (a_ref[...].astype(F32) + b_ref[...].astype(F32))
        for i, (a_ref, b_ref) in enumerate(((a0_ref, b0_ref), (a1_ref, b1_ref)))
    ]
    tile_rows(jnp.concatenate(added, axis=0).astype(BF16), scratch, out_hbm, sems)


def total(*parts):
    return pl.pallas_call(
        total_kernel,
        out_shape=pltpu.HBM((SLOTS * SUB, 128), BF16),
        in_specs=[VMEM] * 5,
        out_specs=HBM,
        scratch_shapes=TILES,
        cost_estimate=cost(400_000_000, 3_000_000),
        name="total",
        compiler_params=LIMIT,
    )(parts[0], *(near(p) for p in parts[1:]))


def combine_kernel(tp_ref, r_ref, route_ref, weight_ref, o_ref, plain):
    tp = tp_ref[0]
    slots = pair_slots(route_ref, tp)
    weights = own_lanes(weight_ref, tp)
    for part in range(3):
        untile_groups(r_ref, range(part * 4, part * 4 + 4), lambda g: (plain, g * 16))
    added = None
    for k in range(2):
        slot = jnp.broadcast_to(column(slots[:, k * TOK : (k + 1) * TOK]), (TOK, SLOTS))
        pick = jnp.where(iota((TOK, SLOTS), 1).astype(F32) == slot, 1.0, 0.0).astype(BF16)
        term = column(weights[k : k + 1]) * dot(pick, plain[...])
        added = term if added is None else added + term
    o_ref[...] = added.astype(BF16)


def combine(tp, back, routes, route_weight):
    return pl.pallas_call(
        combine_kernel,
        in_specs=[SMEM, VMEM, VMEM, VMEM],
        out_specs=VMEM,
        out_shape=jax.ShapeDtypeStruct((TOK, D), BF16),
        scratch_shapes=[pltpu.VMEM((SLOTS, D), BF16)],
        cost_estimate=cost(400_000_000, 2_000_000),
        name="combine",
        compiler_params=LIMIT,
    )(tp, near(back), routes.T, route_weight.T)


def attend_kernel(last, ep_ref, tp_ref, q_ref, gate_ref, blocks_ref, *refs):
    carried, refs = (refs[:3], refs[3:]) if last else ((), refs)
    outs, (best, total, summed, out_ref) = (refs[:4], refs[4:]) if last else ((), refs + (None,))
    me = ep_ref[0]
    plane, row, core = me // 8, (me // 2) % 4, me % 2
    core = 1 - core if last else core
    q = q_ref[...].astype(F32) * 0.125
    q = jnp.concatenate([q[:, :64], q[:, 64:]], axis=0).astype(BF16)
    col = column(gate_ref[:, pl.ds(pl.multiple_of(me * 128, 128), 128)])
    gate_col = jnp.concatenate([col, col], axis=0)

    def blocks_of(z, low, high):
        return jnp.concatenate([blocks_ref[z * 4 + i, low:high, :] for i in range(4)], axis=1)

    def starts_of(z):
        return [((z * 4 + (row + dy + 4) % 4) * 2 + core) * 128 for dy in ROW_OFFSETS]

    def scores_of(z):
        gates = [gate_ref[:, pl.ds(pl.multiple_of(at, 128), 128)] for at in starts_of(z)]
        return dot(q, blocks_of(z, 0, 64)) + gate_col - jnp.concatenate(gates, axis=1)

    def weighted(weights, z):
        return lax.dot_general(
            weights.astype(BF16),
            blocks_of(z, 64, 128),
            (((1,), (1,)), ((), ())),
            preferred_element_type=F32,
        )

    def merge(scores, z, before, count, product):
        top = jnp.maximum(before, jnp.max(scores, axis=1, keepdims=True))
        factor = jnp.exp(before - top)
        weights = jnp.exp(scores - top)
        best[...] = top
        total[...] = count * factor + jnp.sum(weights, axis=1, keepdims=True)
        summed[...] = product * factor + weighted(weights, z)

    scores = scores_of(plane)
    query = iota((256, 128), 0) % 128 + me * 128
    allowed = jnp.concatenate([iota((256, 128), 1) + at <= query for at in starts_of(plane)], axis=1)
    scores = jnp.where(allowed, scores, -jnp.inf)
    if last:
        merge(scores, plane, *(ref[...] for ref in carried))
    else:
        top = jnp.max(scores, axis=1, keepdims=True)
        weights = jnp.exp(scores - top)
        best[...] = top
        total[...] = jnp.sum(weights, axis=1, keepdims=True)
        summed[...] = weighted(weights, plane)

    @pl.loop(0, plane)
    def _(z):
        merge(scores_of(z), z, best[...], total[...], summed[...])

    if last:
        out = summed[...] / total[...]
        out_ref[...] = jnp.concatenate([out[:128], out[128:]], axis=1)
        for ref, shift in zip(outs, TP_SHIFTS):
            at = pl.multiple_of((tp_ref[0] + shift + 4) % 4 * 32, 32)
            ref[...] = out_ref[pl.ds(at, 32), :].astype(BF16)


STATE = ((256, 1), (256, 1), (256, 64))


def attend_same(ep, tp, queries, cum_gate, blocks):
    return pl.pallas_call(
        functools.partial(attend_kernel, False),
        out_shape=[near_out(shape, F32) for shape in STATE],
        in_specs=[SMEM] * 2 + [VMEM] * 3,
        out_specs=[VMEM] * 3,
        cost_estimate=cost(2_000_000_000, 1_500_000),
        name="attend_same",
        compiler_params=LIMIT,
    )(ep, tp, near(queries), near(cum_gate), near(blocks))


def attend_other(ep, tp, queries, cum_gate, blocks, state):
    return pl.pallas_call(
        functools.partial(attend_kernel, True),
        out_shape=[near_out((32, 128))] * 4,
        in_specs=[SMEM] * 2 + [VMEM] * 6,
        out_specs=[VMEM] * 4,
        scratch_shapes=[pltpu.VMEM(shape, F32) for shape in STATE + ((128, 128),)],
        cost_estimate=cost(2_000_000_000, 1_500_000),
        name="attend_other",
        compiler_params=LIMIT,
    )(ep, tp, near(queries), near(cum_gate), near(blocks), *(near(x) for x in state))


def project_kernel(tp_ref, a_ref, b_ref, c_ref, d_ref, w_ref, o_ref):
    added = None
    for ref, shift in zip((a_ref, b_ref, c_ref, d_ref), TP_SHIFTS):
        at = pl.multiple_of((tp_ref[0] - shift + 4) % 4 * 128, 128)
        term = dot(ref[...], w_ref[pl.ds(at, 128), :])
        added = term if added is None else added + term
    o_ref[...] = added.astype(BF16)


def project(tp, parts, out_weight):
    return pl.pallas_call(
        project_kernel,
        out_shape=jax.ShapeDtypeStruct((32, D), BF16),
        in_specs=[SMEM] + [VMEM] * 5,
        out_specs=VMEM,
        cost_estimate=cost(70_000_000, 2_300_000),
        name="project",
        compiler_params=LIMIT,
    )(tp, *(near(p) for p in parts), out_weight)


def over_experts(x):
    return lax.all_to_all(x.reshape(EXPERTS, 48, 128), "ep", 0, 0, tiled=True).reshape(SLOTS * SUB, 128)


def repeat_kernel(a_ref, b_ref, c_ref, d_ref, o_ref):
    for i, ref in enumerate((a_ref, b_ref, c_ref, d_ref)):
        for z in range(Z):
            o_ref[z, i] = ref[...]


def repeated(*blocks):
    return pl.pallas_call(
        repeat_kernel,
        out_shape=pltpu.HBM((Z, 4, 128, 128), BF16),
        in_specs=[VMEM] * 4,
        out_specs=VMEM,
        cost_estimate=cost(1_000_000, 1_200_000),
        name="repeat",
        compiler_params=LIMIT,
    )(*(near(b) for b in blocks))


def over_planes(own):
    return lax.all_to_all(own, "ep", 0, 0, tiled=True, axis_index_groups=PLANES).reshape(32, 128, 128)


def gather_kv(key_cache, value_cache):
    kv = jnp.concatenate([key_cache[0], value_cache[0]], axis=0)
    ring = repeated(
        kv, lax.ppermute(kv, "ep", y_perm(1)), lax.ppermute(kv, "ep", y_perm(-1)), lax.ppermute(kv, "ep", y_perm(2))
    )
    same = over_planes(ring)
    return same, lax.ppermute(same, "ep", core_perm())


def body(
    queries,
    key_cache,
    value_cache,
    cum_gate,
    out_weight,
    routed_input,
    norm_gain,
    routes,
    route_weight,
    expert_gate,
    expert_up,
    expert_down,
):
    tp = lax.axis_index("tp").astype(jnp.int32).reshape(1)
    ep = lax.axis_index("ep").astype(jnp.int32).reshape(1)
    weights = (near(expert_gate), near(expert_up), near(expert_down))
    came = over_experts(prep(tp, routed_input, norm_gain, routes))
    own_top, own_bottom = untile(came)
    left_top = lax.ppermute(own_top, "tp", tp_perm(1))
    right_bottom = lax.ppermute(own_bottom, "tp", tp_perm(-1))
    left_bottom = lax.ppermute(own_bottom, "tp", tp_perm(1))
    right_top = lax.ppermute(own_top, "tp", tp_perm(-1))
    far_top = lax.ppermute(left_top, "tp", tp_perm(1))
    far_bottom = lax.ppermute(right_bottom, "tp", tp_perm(-1))
    (own_part,) = expert_rows(weights, (pltpu.HBM,), own_top, own_bottom)
    left_part_top, left_part_bottom, right_part_top, right_part_bottom = expert_rows(
        weights, (pltpu.VMEM, pltpu.HBM, pltpu.HBM, pltpu.VMEM), left_top, left_bottom, right_top, right_bottom
    )
    far_part_top, far_part_bottom = expert_rows(weights, (pltpu.VMEM,) * 2, far_top, far_bottom)
    from_right_top = lax.ppermute(left_part_top, "tp", tp_perm(-1))
    from_left_bottom = lax.ppermute(right_part_bottom, "tp", tp_perm(1))
    passed_top = lax.ppermute(far_part_top, "tp", tp_perm(1))
    passed_bottom = lax.ppermute(far_part_bottom, "tp", tp_perm(-1))
    right_part_top, left_part_bottom = add_pairs(right_part_top, passed_top, left_part_bottom, passed_bottom)
    from_left_top = lax.ppermute(right_part_top, "tp", tp_perm(1))
    from_right_bottom = lax.ppermute(left_part_bottom, "tp", tp_perm(-1))
    mine = total(own_part, from_right_top, from_left_top, from_left_bottom, from_right_bottom)
    expert_out = combine(tp, over_experts(mine), routes, route_weight)

    same, other = gather_kv(key_cache, value_cache)
    state = attend_same(ep, tp, queries, cum_gate, same)
    rows, up, down, across = attend_other(ep, tp, queries, cum_gate, other, state)
    parts = (
        rows,
        lax.ppermute(up, "tp", tp_perm(1)),
        lax.ppermute(down, "tp", tp_perm(-1)),
        lax.ppermute(across, "tp", tp_perm(2)),
    )
    mixed_out = project(tp, parts, out_weight)
    return (mixed_out, expert_out)


def solution(mesh):
    return jax.shard_map(
        body,
        mesh=mesh,
        in_specs=(
            P("ep", "tp"),
            P("tp", None, "ep"),
            P("tp", None, "ep"),
            P("tp", None),
            P(),
            P("ep", None),
            P(),
            P("ep", None),
            P("ep", None),
            P("ep", None, "tp"),
            P("ep", None, "tp"),
            P("ep", "tp", None),
        ),
        out_specs=(P(("ep", "tp"), None), P(("ep", "tp"), None)),
        check_vma=False,
    )
```

time: 169 us -> 138 us (0.82)
  waiting for transfers between devices: 77.4 us -> 63.4 us
  Pallas kernels: 28.8 us -> 17 us
  local copies, waits for them, and re-layouts: 7.71 us -> 3.18 us
    all_to_all x2 -> x1, waiting for transfers between devices: 24.1 us -> 0.01 us  [over_planes(): lax.all_to_all(own, 'ep', 0, 0, tiled=True, axis_index_groups=PLANES)]
    ppermute x10 -> x15, waiting for transfers between devices: 13.6 us -> 34.4 us  [the longest x1 8.61 us: body(): left_top = lax.ppermute(own_top, 'tp', tp_perm(1))]
    pallas_call x9 -> x12, Pallas kernels: 28.8 us -> 17 us  [the longest x3 5.04 us: expert_rows(): pl.pallas_call(functools.partial(rows_kernel, count), out_shape=[place((r...]
    all_to_all x2, waiting for transfers between devices: 36.6 us -> 25.1 us  [over_experts(): lax.all_to_all(x.reshape(EXPERTS, 48, 128), 'ep', 0, 0, tiled=True)]
    ppermute x10 -> x15, starting transfers between devices: 13.5 us -> 19.9 us  [the longest x1 2.76 us: body(): lax.ppermute(down, 'tp', tp_perm(-1))]
    all_to_all x2 -> x1, starting transfers between devices: 7.5 us -> 4.25 us  [over_planes(): lax.all_to_all(own, 'ep', 0, 0, tiled=True, axis_index_groups=PLANES)]
    all_to_all x2, starting transfers between devices: 26.1 us -> 24 us  [over_experts(): lax.all_to_all(x.reshape(EXPERTS, 48, 128), 'ep', 0, 0, tiled=True)]
    reshape x2 -> x0, local copies, waits for them, and re-layouts: 2 us -> none  [the longest x1 1.29 us: prep(): gain.reshape(1, D)]
  transfers between devices with their start and end apart: 18 -> 22, of which waited for: 10 -> 14; matrix products, arithmetic and copies ran while one was open for 2% -> 0% of each run, Pallas kernels for 14% -> 9%
where the time goes in v2:
time: 138 us
  waiting for transfers between devices  63.4 us (46%)
  starting transfers between devices  53.2 us (39%)
  Pallas kernels  17 us (12%)
  local copies, waits for them, and re-layouts  3.18 us (2%)
    all_to_all x2, waiting for transfers between devices, over_experts(): lax.all_to_all(x.reshape(EXPERTS, 48, 128), 'ep', 0, 0, tiled=True)  25.1 us
    all_to_all x2, starting transfers between devices, over_experts(): lax.all_to_all(x.reshape(EXPERTS, 48, 128), 'ep', 0, 0, tiled=True)  24 us
    ppermute x1, waiting for transfers between devices, body(): left_top = lax.ppermute(own_top, 'tp', tp_perm(1))  8.61 us
    ppermute x1, waiting for transfers between devices, body(): from_left_top = lax.ppermute(right_part_top, 'tp', tp_perm(1))  7.53 us
    ppermute x1, waiting for transfers between devices, body(): far_top = lax.ppermute(left_top, 'tp', tp_perm(1))  5.07 us
    pallas_call x3, Pallas kernels, expert_rows(): pl.pallas_call(functools.partial(rows_kernel, count), out_shape=[place((r...  5.04 us
    ppermute x1, waiting for transfers between devices, body(): left_bottom = lax.ppermute(own_bottom, 'tp', tp_perm(1))  4.74 us
    all_to_all x1, starting transfers between devices, over_planes(): lax.all_to_all(own, 'ep', 0, 0, tiled=True, axis_index_groups=PLANES)  4.25 us
  transfers between devices with their start and end apart: 22, of which 14 were waited for; matrix products, arithmetic and copies ran while one was open for 0% of the time, Pallas kernels for 9%

profile of v2, /device:TPU:1, one launch (start us, length us, event | category | flops | bytes accessed | tf_op | source)
XLA Modules:
  0.0 137.6 jit_solution(13490862990081630739)
XLA Ops:
  0.7 2.6 %prep.1 = bf16[3072,128]{1,0:T(8,128)(2,1)} custom-call(s32[1]{0:T(128)} %bitcast.tp_ref, bf16[256,2048]{1,0:T(8,128)(2,1)} %x_hbm.1, bf16[2048]{0:T(1024)(128)(2,1)} %gain_hbm.1, s32[2,256]{1,0:T(2,128)} %bitcast.12), custom_call_target="tpu_custom_call" | custom-call | flops 400000000 | bytes 2000000 | tf_op jit(solution)/shard_map/prep/pallas_call | solution.py:146
  3.3 13.3 %all-to-all-start.1 = ((bf16[64,48,128]{2,1,0:T(8,128)(2,1)}), bf16[64,48,128]{2,1,0:T(8,128)(2,1)}, u32[]{:S(2)}, u32[]{:S(2)}) async-start(bf16[64,48,128]{2,1,0:T(8,128)(2,1)} %bitcast.15), calls=%async_computation.1 | async-start | bytes 1572864 | tf_op jit(solution)/shard_map/all_to_all | solution.py:396
  16.7 1.4 %collective-permute-start = (bf16[128,128]{1,0:T(8,128)(2,1)S(1)}, bf16[128,128]{1,0:T(8,128)(2,1)S(1)}, u32[]{:S(2)}, u32[]{:S(2)}) collective-permute-start(bf16[128,128]{1,0:T(8,128)(2,1)S(1)} %pad_maximum_fusion.a_ref), channel_id=1, source_target_pairs={{0,8},{4,12},{8,16},{12,20},{16,24},{20,28},{24,0},{28,4},{32,40},... | collective-permute-start | bytes 98312 | tf_op jit(solution)/shard_map/ppermute | solution.py:424
  18.1 1.3 collective-permute-start.1
  19.4 1.6 %collective-permute-start.2 = (bf16[128,128]{1,0:T(8,128)(2,1)S(1)}, bf16[128,128]{1,0:T(8,128)(2,1)S(1)}, u32[]{:S(2)}, u32[]{:S(2)}) collective-permute-start(bf16[128,128]{1,0:T(8,128)(2,1)S(1)} %pad_maximum_fusion.a_ref), channel_id=1, source_target_pairs={{0,16},{4,20},{8,24},{12,28},{16,0},{20,4},{24,8},{28,12},{32,48},... | collective-permute-start | bytes 98312 | tf_op jit(solution)/shard_map/ppermute | solution.py:424
  21.1 0.7 collective-permute-done.b_ref
  21.8 2.4 %collective-permute-done.2.d_ref = bf16[128,128]{1,0:T(8,128)(2,1)S(1)} collective-permute-done((bf16[128,128]{1,0:T(8,128)(2,1)S(1)}, bf16[128,128]{1,0:T(8,128)(2,1)S(1)}, u32[]{:S(2)}, u32[]{:S(2)}) %collective-permute-start.2) | collective-permute-done | bytes 32800 | tf_op jit(solution)/shard_map/ppermute | solution.py:424
  24.1 1.1 repeat.1
  25.3 14.3 %all-to-all-done.1 = bf16[64,48,128]{2,1,0:T(8,128)(2,1)} async-done(((bf16[64,48,128]{2,1,0:T(8,128)(2,1)}), bf16[64,48,128]{2,1,0:T(8,128)(2,1)}, u32[]{:S(2)}, u32[]{:S(2)}) %all-to-all-start.1) | async-done | bytes 786464 | tf_op jit(solution)/shard_map/all_to_all | solution.py:396
  39.5 4.3 %all-to-all-start = ((bf16[8,4,128,128]{3,2,1,0:T(8,128)(2,1)}), bf16[8,4,128,128]{3,2,1,0:T(8,128)(2,1)}, u32[]{:S(2)}, u32[]{:S(2)}) async-start(bf16[8,4,128,128]{3,2,1,0:T(8,128)(2,1)} %repeat.1), calls=%async_computation | async-start | bytes 2097152 | tf_op jit(solution)/shard_map/all_to_all | solution.py:418
  43.8 1.7 %untile.1 = (bf16[96,2048]{1,0:T(8,128)(2,1)S(1)}, bf16[96,2048]{1,0:T(8,128)(2,1)S(1)}) custom-call(bf16[3072,128]{1,0:T(8,128)(2,1)} %bitcast.7.a_hbm), custom_call_target="tpu_custom_call" | custom-call | flops 400000000 | bytes 1600000 | tf_op jit(solution)/shard_map/untile/pallas_call | solution.py:180
  45.5 1.3 collective-permute-start.7
  46.8 1.5 %collective-permute-start.10 = (bf16[96,2048]{1,0:T(8,128)(2,1)S(1)}, bf16[96,2048]{1,0:T(8,128)(2,1)S(1)}, u32[]{:S(2)}, u32[]{:S(2)}) collective-permute-start(bf16[96,2048]{1,0:T(8,128)(2,1)S(1)} %get-tuple-element.27.refs_1_), channel_id=1, source_target_pairs={{0,3},{1,0},{2,1},{3,2},{4,7},{5,4},{6,5},{7,6},{8,11},{9,8},{10,9... | collective-permute-start | bytes 1179656 | tf_op jit(solution)/shard_map/ppermute | solution.py:450
  48.2 8.6 %collective-permute-done.7.refs_0_ = bf16[96,2048]{1,0:T(8,128)(2,1)S(1)} collective-permute-done((bf16[96,2048]{1,0:T(8,128)(2,1)S(1)}, bf16[96,2048]{1,0:T(8,128)(2,1)S(1)}, u32[]{:S(2)}, u32[]{:S(2)}) %collective-permute-start.7) | collective-permute-done | bytes 393248 | tf_op jit(solution)/shard_map/ppermute | solution.py:449
  56.8 2.7 %collective-permute-start.13 = (bf16[96,2048]{1,0:T(8,128)(2,1)S(1)}, bf16[96,2048]{1,0:T(8,128)(2,1)S(1)}, u32[]{:S(2)}, u32[]{:S(2)}) collective-permute-start(bf16[96,2048]{1,0:T(8,128)(2,1)S(1)} %collective-permute-done.10.refs_3_), channel_id=1, source_target_pairs={{0,3},{1,0},{2,1},{3,2},{4,7},{5,4},{6,5},{7,6},{8,11},{9,8},{10,9... | collective-permute-start | bytes 1179656 | tf_op jit(solution)/shard_map/ppermute | solution.py:454
  59.5 2.7 %collective-permute-start.9 = (bf16[96,2048]{1,0:T(8,128)(2,1)S(1)}, bf16[96,2048]{1,0:T(8,128)(2,1)S(1)}, u32[]{:S(2)}, u32[]{:S(2)}) collective-permute-start(bf16[96,2048]{1,0:T(8,128)(2,1)S(1)} %get-tuple-element.26.refs_0_), channel_id=1, source_target_pairs={{0,3},{1,0},{2,1},{3,2},{4,7},{5,4},{6,5},{7,6},{8,11},{9,8},{10,9... | collective-permute-start | bytes 1179656 | tf_op jit(solution)/shard_map/ppermute | solution.py:452
  62.2 5.1 %collective-permute-done.12.refs_0_ = bf16[96,2048]{1,0:T(8,128)(2,1)S(1)} collective-permute-done((bf16[96,2048]{1,0:T(8,128)(2,1)S(1)}, bf16[96,2048]{1,0:T(8,128)(2,1)S(1)}, u32[]{:S(2)}, u32[]{:S(2)}) %collective-permute-start.12) | collective-permute-done | bytes 393248 | tf_op jit(solution)/shard_map/ppermute | solution.py:453
  67.3 0.9 expert_rows.5
  68.2 0.1 collective-permute-start.14
  68.3 2.7 %collective-permute-start.15 = (bf16[96,2048]{1,0:T(8,128)(2,1)S(1)}, bf16[96,2048]{1,0:T(8,128)(2,1)S(1)}, u32[]{:S(2)}, u32[]{:S(2)}) collective-permute-start(bf16[96,2048]{1,0:T(8,128)(2,1)S(1)} %get-tuple-element.32), channel_id=1, source_target_pairs={{0,3},{1,0},{2,1},{3,2},{4,7},{5,4},{6,5},{7,6},{8,11},{9,8},{10,9... | collective-permute-start | bytes 1179656 | tf_op jit(solution)/shard_map/ppermute | solution.py:463
  71.0 4.7 %collective-permute-done.8.refs_1_ = bf16[96,2048]{1,0:T(8,128)(2,1)S(1)} collective-permute-done((bf16[96,2048]{1,0:T(8,128)(2,1)S(1)}, bf16[96,2048]{1,0:T(8,128)(2,1)S(1)}, u32[]{:S(2)}, u32[]{:S(2)}) %collective-permute-start.8) | collective-permute-done | bytes 393248 | tf_op jit(solution)/shard_map/ppermute | solution.py:451
  75.7 2.3 %expert_rows.4 = (bf16[96,2048]{1,0:T(8,128)(2,1)S(1)}, bf16[96,2048]{1,0:T(8,128)(2,1)}, bf16[96,2048]{1,0:T(8,128)(2,1)}, bf16[96,2048]{1,0:T(8,128)(2,1)S(1)}) custom-call(bf16[96,2048]{1,0:T(8,128)(2,1)S(1)} %collective-permute-done.7.refs_0_, bf16[96,2048]{1,0:T(8,128)(2,1)S(1)} %collective-permute-done.8.refs_1_, ...), custom_call_target="tpu_custom_call" | custom-call | flops 1152000000 | bytes 3072000 | tf_op jit(solution)/shard_map/expert_rows/pallas_call | solution.py:207
  78.0 2.4 %collective-permute-start.11 = (bf16[96,2048]{1,0:T(8,128)(2,1)S(1)}, bf16[96,2048]{1,0:T(8,128)(2,1)S(1)}, u32[]{:S(2)}, u32[]{:S(2)}) collective-permute-start(bf16[96,2048]{1,0:T(8,128)(2,1)S(1)} %get-tuple-element.28), channel_id=1, source_target_pairs={{0,3},{1,0},{2,1},{3,2},{4,7},{5,4},{6,5},{7,6},{8,11},{9,8},{10,9... | collective-permute-start | bytes 1179656 | tf_op jit(solution)/shard_map/ppermute | solution.py:460
  80.4 3.7 %collective-permute-done.14.b_ref = bf16[96,2048]{1,0:T(8,128)(2,1)S(1)} collective-permute-done((bf16[96,2048]{1,0:T(8,128)(2,1)S(1)}, bf16[96,2048]{1,0:T(8,128)(2,1)S(1)}, u32[]{:S(2)}, u32[]{:S(2)}) %collective-permute-start.14) | collective-permute-done | bytes 393248 | tf_op jit(solution)/shard_map/ppermute | solution.py:462
  84.1 1.0 copy-done.5
  85.1 1.0 copy-done.6
  86.1 0.2 add_pairs.1
  86.3 0.1 collective-permute-start.16
  86.4 2.7 %collective-permute-start.18 = (bf16[96,2048]{1,0:T(8,128)(2,1)S(1)}, bf16[96,2048]{1,0:T(8,128)(2,1)S(1)}, u32[]{:S(2)}, u32[]{:S(2)}) collective-permute-start(bf16[96,2048]{1,0:T(8,128)(2,1)S(1)} %get-tuple-element.35), channel_id=1, source_target_pairs={{0,3},{1,0},{2,1},{3,2},{4,7},{5,4},{6,5},{7,6},{8,11},{9,8},{10,9... | collective-permute-start | bytes 1179656 | tf_op jit(solution)/shard_map/ppermute | solution.py:466
  89.1 1.8 %expert_rows.3.own_ref = bf16[192,2048]{1,0:T(8,128)(2,1)} custom-call(bf16[96,2048]{1,0:T(8,128)(2,1)S(1)} %get-tuple-element.26.refs_0_, bf16[96,2048]{1,0:T(8,128)(2,1)S(1)} %get-tuple-element.27.refs_1_, bf16[1,2048,256]{2,1,0:T(8,128)(2,1)S(1)} %copy-done, bf16[1,2048,256]{2,1,0:T(8,128)(2,1)S(1)} %copy-done.1, bf16[1,256,2048]{2,1,0:T(8,128)(2,1)S(1)} %copy-done.2), custom_call_target="tpu_custom_call" | custom-call | flops 576000000 | bytes 1536000 | tf_op jit(solution)/shard_map/expert_rows/pallas_call | solution.py:207
  90.9 0.7 collective-permute-done.11.a0_ref
  91.5 7.5 %collective-permute-done.16.b0_ref = bf16[96,2048]{1,0:T(8,128)(2,1)S(1)} collective-permute-done((bf16[96,2048]{1,0:T(8,128)(2,1)S(1)}, bf16[96,2048]{1,0:T(8,128)(2,1)S(1)}, u32[]{:S(2)}, u32[]{:S(2)}) %collective-permute-start.16) | collective-permute-done | bytes 393248 | tf_op jit(solution)/shard_map/ppermute | solution.py:465
  99.1 0.9 collective-permute-done.18.b1_ref
  100.0 1.1 copy-done.3
  101.1 1.3 total.1
  102.4 10.7 %all-to-all-start.2 = ((bf16[64,48,128]{2,1,0:T(8,128)(2,1)}), bf16[64,48,128]{2,1,0:T(8,128)(2,1)S(1)}, u32[]{:S(2)}, u32[]{:S(2)}) async-start(bf16[64,48,128]{2,1,0:T(8,128)(2,1)} %bitcast.16), calls=%async_computation.2 | async-start | bytes 1572864 | tf_op jit(solution)/shard_map/all_to_all | solution.py:396
  113.1 0.5 collective-permute-start.3
  113.7 1.7 %attend_same.1 = (f32[256,1]{1,0:T(8,128)S(1)}, f32[256,1]{1,0:T(8,128)S(1)}, f32[256,64]{1,0:T(8,128)S(1)}) custom-call(s32[1]{0:T(128)} %bitcast.1.ep_ref, s32[1]{0:T(128)} %bitcast.tp_ref, bf16[128,128]{1,0:T(8,128)(2,1)S(1)} %copy-done.8, f32[1,8192]{1,0:T(1,128)S(1)} %copy-done.9, bf16[32,128,128]{2,1,0:T(8,128)(2,1)} %bitcast.4.blocks_ref), custom_call_target="tpu_custom_call" | custom-call | flops 2000000000 | bytes 1500000 | tf_op jit(solution)/shard_map/attend_same/pallas_call | solution.py:350
  115.4 0.8 collective-permute-done.3.blocks_ref
  116.2 0.9 attend_other.1
  117.1 0.1 collective-permute-start.4
  117.2 2.8 %collective-permute-start.5 = (bf16[32,128]{1,0:T(8,128)(2,1)S(1)}, bf16[32,128]{1,0:T(8,128)(2,1)S(1)}, u32[]{:S(2)}, u32[]{:S(2)}) collective-permute-start(bf16[32,128]{1,0:T(8,128)(2,1)S(1)} %get-tuple-element.24), channel_id=1, source_target_pairs={{0,3},{1,0},{2,1},{3,2},{4,7},{5,4},{6,5},{7,6},{8,11},{9,8},{10,9... | collective-permute-start | bytes 24584 | tf_op jit(solution)/shard_map/ppermute | solution.py:476
  119.9 1.1 collective-permute-start.6
  121.0 0.1 collective-permute-done.4.b_ref
  121.2 3.1 %collective-permute-done.6.d_ref = bf16[32,128]{1,0:T(8,128)(2,1)S(1)} collective-permute-done((bf16[32,128]{1,0:T(8,128)(2,1)S(1)}, bf16[32,128]{1,0:T(8,128)(2,1)S(1)}, u32[]{:S(2)}, u32[]{:S(2)}) %collective-permute-start.6) | collective-permute-done | bytes 8224 | tf_op jit(solution)/shard_map/ppermute | solution.py:477
  124.2 1.1 project.1
  125.3 10.8 %all-to-all-done.2 = bf16[64,48,128]{2,1,0:T(8,128)(2,1)S(1)} async-done(((bf16[64,48,128]{2,1,0:T(8,128)(2,1)}), bf16[64,48,128]{2,1,0:T(8,128)(2,1)S(1)}, u32[]{:S(2)}, u32[]{:S(2)}) %all-to-all-start.2) | async-done | bytes 786464 | tf_op jit(solution)/shard_map/all_to_all | solution.py:396
  136.1 1.4 %combine.1 = bf16[64,2048]{1,0:T(8,128)(2,1)} custom-call(s32[1]{0:T(128)} %bitcast.tp_ref, bf16[3072,128]{1,0:T(8,128)(2,1)S(1)} %bitcast.11, s32[2,256]{1,0:T(2,128)S(1)} %bitcast.13, f32[2,256]{1,0:T(2,128)S(1)} %bitcast.14), custom_call_target="tpu_custom_call" | custom-call | flops 400000000 | bytes 2000000 | tf_op jit(solution)/shard_map/combine/pallas_call | solution.py:272
  (35 shorter events, 0.1 us)
Async XLA Ops:
  0.6 16.0 %copy-start.12 = (bf16[1,64,128]{2,1,0:T(8,128)(2,1)S(1)}, bf16[1,64,128]{2,1,0:T(8,128)(2,1)}, u32[]{:S(2)}) copy-start(bf16[1,64,128]{2,1,0:T(8,128)(2,1)} %param.13) | copy-start | bytes 49156
  0.6 16.0 %copy-start.11 = (bf16[1,64,128]{2,1,0:T(8,128)(2,1)S(1)}, bf16[1,64,128]{2,1,0:T(8,128)(2,1)}, u32[]{:S(2)}) copy-start(bf16[1,64,128]{2,1,0:T(8,128)(2,1)} %param.14) | copy-start | bytes 49156
  3.3 36.3 %all-to-all-start.1 = ((bf16[64,48,128]{2,1,0:T(8,128)(2,1)}), bf16[64,48,128]{2,1,0:T(8,128)(2,1)}, u32[]{:S(2)}, u32[]{:S(2)}) async-start(bf16[64,48,128]{2,1,0:T(8,128)(2,1)} %bitcast.15), calls=%async_computation.1 | async-start | bytes 1572864 | tf_op jit(solution)/shard_map/all_to_all | solution.py:396
  16.6 50.6 %copy-start = (bf16[1,2048,256]{2,1,0:T(8,128)(2,1)S(1)}, bf16[1,2048,256]{2,1,0:T(8,128)(2,1)}, u32[]{:S(2)}) copy-start(bf16[1,2048,256]{2,1,0:T(8,128)(2,1)} %refs_2_.3) | copy-start | bytes 3145732
  16.6 50.6 %copy-start.1 = (bf16[1,2048,256]{2,1,0:T(8,128)(2,1)S(1)}, bf16[1,2048,256]{2,1,0:T(8,128)(2,1)}, u32[]{:S(2)}) copy-start(bf16[1,2048,256]{2,1,0:T(8,128)(2,1)} %refs_3_.3) | copy-start | bytes 3145732
  16.7 50.6 %copy-start.2 = (bf16[1,256,2048]{2,1,0:T(8,128)(2,1)S(1)}, bf16[1,256,2048]{2,1,0:T(8,128)(2,1)}, u32[]{:S(2)}) copy-start(bf16[1,256,2048]{2,1,0:T(8,128)(2,1)} %refs_4_.5) | copy-start | bytes 3145732
  16.7 5.1 %collective-permute-start = (bf16[128,128]{1,0:T(8,128)(2,1)S(1)}, bf16[128,128]{1,0:T(8,128)(2,1)S(1)}, u32[]{:S(2)}, u32[]{:S(2)}) collective-permute-start(bf16[128,128]{1,0:T(8,128)(2,1)S(1)} %pad_maximum_fusion.a_ref), channel_id=1, source_target_pairs={{0,8},{4,12},{8,16},{12,20},{16,24},{20,28},{24,0},{28,4},{32,40},... | collective-permute-start | bytes 98312 | tf_op jit(solution)/shard_map/ppermute | solution.py:424
  18.1 3.7 %collective-permute-start.1 = (bf16[128,128]{1,0:T(8,128)(2,1)S(1)}, bf16[128,128]{1,0:T(8,128)(2,1)S(1)}, u32[]{:S(2)}, u32[]{:S(2)}) collective-permute-start(bf16[128,128]{1,0:T(8,128)(2,1)S(1)} %pad_maximum_fusion.a_ref), channel_id=1, source_target_pairs={{0,24},{4,28},{8,0},{12,4},{16,8},{20,12},{24,16},{28,20},{32,56},... | collective-permute-start | bytes 98312 | tf_op jit(solution)/shard_map/ppermute | solution.py:424
  19.4 4.7 %collective-permute-start.2 = (bf16[128,128]{1,0:T(8,128)(2,1)S(1)}, bf16[128,128]{1,0:T(8,128)(2,1)S(1)}, u32[]{:S(2)}, u32[]{:S(2)}) collective-permute-start(bf16[128,128]{1,0:T(8,128)(2,1)S(1)} %pad_maximum_fusion.a_ref), channel_id=1, source_target_pairs={{0,16},{4,20},{8,24},{12,28},{16,0},{20,4},{24,8},{28,12},{32,48},... | collective-permute-start | bytes 98312 | tf_op jit(solution)/shard_map/ppermute | solution.py:424
  39.5 62.9 %all-to-all-start = ((bf16[8,4,128,128]{3,2,1,0:T(8,128)(2,1)}), bf16[8,4,128,128]{3,2,1,0:T(8,128)(2,1)}, u32[]{:S(2)}, u32[]{:S(2)}) async-start(bf16[8,4,128,128]{3,2,1,0:T(8,128)(2,1)} %repeat.1), calls=%async_computation | async-start | bytes 2097152 | tf_op jit(solution)/shard_map/all_to_all | solution.py:418
  45.5 11.4 %collective-permute-start.7 = (bf16[96,2048]{1,0:T(8,128)(2,1)S(1)}, bf16[96,2048]{1,0:T(8,128)(2,1)S(1)}, u32[]{:S(2)}, u32[]{:S(2)}) collective-permute-start(bf16[96,2048]{1,0:T(8,128)(2,1)S(1)} %get-tuple-element.26.refs_0_), channel_id=1, source_target_pairs={{0,1},{1,2},{2,3},{3,0},{4,5},{5,6},{6,7},{7,4},{8,9},{9,10},{10,1... | collective-permute-start | bytes 1179656 | tf_op jit(solution)/shard_map/ppermute | solution.py:449
  46.8 10.1 %collective-permute-start.10 = (bf16[96,2048]{1,0:T(8,128)(2,1)S(1)}, bf16[96,2048]{1,0:T(8,128)(2,1)S(1)}, u32[]{:S(2)}, u32[]{:S(2)}) collective-permute-start(bf16[96,2048]{1,0:T(8,128)(2,1)S(1)} %get-tuple-element.27.refs_1_), channel_id=1, source_target_pairs={{0,3},{1,0},{2,1},{3,2},{4,7},{5,4},{6,5},{7,6},{8,11},{9,8},{10,9... | collective-permute-start | bytes 1179656 | tf_op jit(solution)/shard_map/ppermute | solution.py:450
  56.8 10.4 %collective-permute-start.12 = (bf16[96,2048]{1,0:T(8,128)(2,1)S(1)}, bf16[96,2048]{1,0:T(8,128)(2,1)S(1)}, u32[]{:S(2)}, u32[]{:S(2)}) collective-permute-start(bf16[96,2048]{1,0:T(8,128)(2,1)S(1)} %collective-permute-done.7.refs_0_), channel_id=1, source_target_pairs={{0,1},{1,2},{2,3},{3,0},{4,5},{5,6},{6,7},{7,4},{8,9},{9,10},{10,1... | collective-permute-start | bytes 1179656 | tf_op jit(solution)/shard_map/ppermute | solution.py:453
  56.8 10.4 %collective-permute-start.13 = (bf16[96,2048]{1,0:T(8,128)(2,1)S(1)}, bf16[96,2048]{1,0:T(8,128)(2,1)S(1)}, u32[]{:S(2)}, u32[]{:S(2)}) collective-permute-start(bf16[96,2048]{1,0:T(8,128)(2,1)S(1)} %collective-permute-done.10.refs_3_), channel_id=1, source_target_pairs={{0,3},{1,0},{2,1},{3,2},{4,7},{5,4},{6,5},{7,6},{8,11},{9,8},{10,9... | collective-permute-start | bytes 1179656 | tf_op jit(solution)/shard_map/ppermute | solution.py:454
  59.5 16.2 %collective-permute-start.8 = (bf16[96,2048]{1,0:T(8,128)(2,1)S(1)}, bf16[96,2048]{1,0:T(8,128)(2,1)S(1)}, u32[]{:S(2)}, u32[]{:S(2)}) collective-permute-start(bf16[96,2048]{1,0:T(8,128)(2,1)S(1)} %get-tuple-element.27.refs_1_), channel_id=1, source_target_pairs={{0,1},{1,2},{2,3},{3,0},{4,5},{5,6},{6,7},{7,4},{8,9},{9,10},{10,1... | collective-permute-start | bytes 1179656 | tf_op jit(solution)/shard_map/ppermute | solution.py:451
  59.5 16.2 %collective-permute-start.9 = (bf16[96,2048]{1,0:T(8,128)(2,1)S(1)}, bf16[96,2048]{1,0:T(8,128)(2,1)S(1)}, u32[]{:S(2)}, u32[]{:S(2)}) collective-permute-start(bf16[96,2048]{1,0:T(8,128)(2,1)S(1)} %get-tuple-element.26.refs_0_), channel_id=1, source_target_pairs={{0,3},{1,0},{2,1},{3,2},{4,7},{5,4},{6,5},{7,6},{8,11},{9,8},{10,9... | collective-permute-start | bytes 1179656 | tf_op jit(solution)/shard_map/ppermute | solution.py:452
  68.2 15.9 %collective-permute-start.14 = (bf16[96,2048]{1,0:T(8,128)(2,1)S(1)}, bf16[96,2048]{1,0:T(8,128)(2,1)S(1)}, u32[]{:S(2)}, u32[]{:S(2)}) collective-permute-start(bf16[96,2048]{1,0:T(8,128)(2,1)S(1)} %get-tuple-element.30), channel_id=1, source_target_pairs={{0,1},{1,2},{2,3},{3,0},{4,5},{5,6},{6,7},{7,4},{8,9},{9,10},{10,1... | collective-permute-start | bytes 1179656 | tf_op jit(solution)/shard_map/ppermute | solution.py:462
  68.3 15.8 %collective-permute-start.15 = (bf16[96,2048]{1,0:T(8,128)(2,1)S(1)}, bf16[96,2048]{1,0:T(8,128)(2,1)S(1)}, u32[]{:S(2)}, u32[]{:S(2)}) collective-permute-start(bf16[96,2048]{1,0:T(8,128)(2,1)S(1)} %get-tuple-element.32), channel_id=1, source_target_pairs={{0,3},{1,0},{2,1},{3,2},{4,7},{5,4},{6,5},{7,6},{8,11},{9,8},{10,9... | collective-permute-start | bytes 1179656 | tf_op jit(solution)/shard_map/ppermute | solution.py:463
  78.0 13.5 %collective-permute-start.11 = (bf16[96,2048]{1,0:T(8,128)(2,1)S(1)}, bf16[96,2048]{1,0:T(8,128)(2,1)S(1)}, u32[]{:S(2)}, u32[]{:S(2)}) collective-permute-start(bf16[96,2048]{1,0:T(8,128)(2,1)S(1)} %get-tuple-element.28), channel_id=1, source_target_pairs={{0,3},{1,0},{2,1},{3,2},{4,7},{5,4},{6,5},{7,6},{8,11},{9,8},{10,9... | collective-permute-start | bytes 1179656 | tf_op jit(solution)/shard_map/ppermute | solution.py:460
  80.4 11.1 %collective-permute-start.17 = (bf16[96,2048]{1,0:T(8,128)(2,1)S(1)}, bf16[96,2048]{1,0:T(8,128)(2,1)S(1)}, u32[]{:S(2)}, u32[]{:S(2)}) collective-permute-start(bf16[96,2048]{1,0:T(8,128)(2,1)S(1)} %get-tuple-element.34), channel_id=1, source_target_pairs={{0,1},{1,2},{2,3},{3,0},{4,5},{5,6},{6,7},{7,4},{8,9},{9,10},{10,1... | collective-permute-start | bytes 1179656 | tf_op jit(solution)/shard_map/ppermute | solution.py:461
  84.1 1.0 copy-start.5
  85.1 1.0 copy-start.6
  86.3 12.8 %collective-permute-start.16 = (bf16[96,2048]{1,0:T(8,128)(2,1)S(1)}, bf16[96,2048]{1,0:T(8,128)(2,1)S(1)}, u32[]{:S(2)}, u32[]{:S(2)}) collective-permute-start(bf16[96,2048]{1,0:T(8,128)(2,1)S(1)} %get-tuple-element.33), channel_id=1, source_target_pairs={{0,1},{1,2},{2,3},{3,0},{4,5},{5,6},{6,7},{7,4},{8,9},{9,10},{10,1... | collective-permute-start | bytes 1179656 | tf_op jit(solution)/shard_map/ppermute | solution.py:465
  86.4 13.6 %collective-permute-start.18 = (bf16[96,2048]{1,0:T(8,128)(2,1)S(1)}, bf16[96,2048]{1,0:T(8,128)(2,1)S(1)}, u32[]{:S(2)}, u32[]{:S(2)}) collective-permute-start(bf16[96,2048]{1,0:T(8,128)(2,1)S(1)} %get-tuple-element.35), channel_id=1, source_target_pairs={{0,3},{1,0},{2,1},{3,2},{4,7},{5,4},{6,5},{7,6},{8,11},{9,8},{10,9... | collective-permute-start | bytes 1179656 | tf_op jit(solution)/shard_map/ppermute | solution.py:466
  89.1 24.6 %copy-start.8 = (bf16[128,128]{1,0:T(8,128)(2,1)S(1)}, bf16[128,128]{1,0:T(8,128)(2,1)}, u32[]{:S(2)}) copy-start(bf16[128,128]{1,0:T(8,128)(2,1)} %q_ref.3) | copy-start | bytes 98308
  89.1 24.6 %copy-start.9 = (f32[1,8192]{1,0:T(1,128)S(1)}, f32[1,8192]{1,0:T(1,128)}, u32[]{:S(2)}) copy-start(f32[1,8192]{1,0:T(1,128)} %gate_ref.3) | copy-start | bytes 98308
  100.0 1.1 copy-start.3
  102.4 33.7 %all-to-all-start.2 = ((bf16[64,48,128]{2,1,0:T(8,128)(2,1)}), bf16[64,48,128]{2,1,0:T(8,128)(2,1)S(1)}, u32[]{:S(2)}, u32[]{:S(2)}) async-start(bf16[64,48,128]{2,1,0:T(8,128)(2,1)} %bitcast.16), calls=%async_computation.2 | async-start | bytes 1572864 | tf_op jit(solution)/shard_map/all_to_all | solution.py:396
  113.1 3.0 %collective-permute-start.3 = (bf16[32,128,128]{2,1,0:T(8,128)(2,1)}, bf16[32,128,128]{2,1,0:T(8,128)(2,1)S(1)}, u32[]{:S(2)}, u32[]{:S(2)}) collective-permute-start(bf16[32,128,128]{2,1,0:T(8,128)(2,1)} %bitcast.4.blocks_ref), channel_id=1, source_target_pairs={{0,4},{4,0},{8,12},{12,8},{16,20},{20,16},{24,28},{28,24},{32,36},... | collective-permute-start | bytes 3145736 | tf_op jit(solution)/shard_map/ppermute | solution.py:427
  116.2 8.0 %copy-start.4 = (bf16[512,2048]{1,0:T(8,128)(2,1)S(1)}, bf16[512,2048]{1,0:T(8,128)(2,1)}, u32[]{:S(2)}) copy-start(bf16[512,2048]{1,0:T(8,128)(2,1)} %w_ref.1) | copy-start | bytes 6291460
  117.0 19.1 %copy-start.7 = (s32[256,2]{0,1:T(2,128)S(1)}, s32[256,2]{0,1:T(2,128)}, u32[]{:S(2)}) copy-start(s32[256,2]{0,1:T(2,128)} %param.19) | copy-start | bytes 6148
  117.1 19.1 %copy-start.10 = (f32[256,2]{0,1:T(2,128)S(1)}, f32[256,2]{0,1:T(2,128)}, u32[]{:S(2)}) copy-start(f32[256,2]{0,1:T(2,128)} %param.20) | copy-start | bytes 6148
  117.1 4.1 %collective-permute-start.4 = (bf16[32,128]{1,0:T(8,128)(2,1)S(1)}, bf16[32,128]{1,0:T(8,128)(2,1)S(1)}, u32[]{:S(2)}, u32[]{:S(2)}) collective-permute-start(bf16[32,128]{1,0:T(8,128)(2,1)S(1)} %get-tuple-element.23), channel_id=1, source_target_pairs={{0,1},{1,2},{2,3},{3,0},{4,5},{5,6},{6,7},{7,4},{8,9},{9,10},{10,1... | collective-permute-start | bytes 24584 | tf_op jit(solution)/shard_map/ppermute | solution.py:475
  117.2 4.0 %collective-permute-start.5 = (bf16[32,128]{1,0:T(8,128)(2,1)S(1)}, bf16[32,128]{1,0:T(8,128)(2,1)S(1)}, u32[]{:S(2)}, u32[]{:S(2)}) collective-permute-start(bf16[32,128]{1,0:T(8,128)(2,1)S(1)} %get-tuple-element.24), channel_id=1, source_target_pairs={{0,3},{1,0},{2,1},{3,2},{4,7},{5,4},{6,5},{7,6},{8,11},{9,8},{10,9... | collective-permute-start | bytes 24584 | tf_op jit(solution)/shard_map/ppermute | solution.py:476
  119.9 4.3 %collective-permute-start.6 = (bf16[32,128]{1,0:T(8,128)(2,1)S(1)}, bf16[32,128]{1,0:T(8,128)(2,1)S(1)}, u32[]{:S(2)}, u32[]{:S(2)}) collective-permute-start(bf16[32,128]{1,0:T(8,128)(2,1)S(1)} %get-tuple-element.25), channel_id=1, source_target_pairs={{0,2},{1,3},{2,0},{3,1},{4,6},{5,7},{6,4},{7,5},{8,10},{9,11},{10,... | collective-permute-start | bytes 24584 | tf_op jit(solution)/shard_map/ppermute | solution.py:477

commit v3 on v2

--- a/solution.py
+++ b/solution.py
@@ -16,6 +16,7 @@
 D = 2048
 SUB = 16
 TOP = 96
+QUARTER = 48
 F32 = jnp.float32
 BF16 = jnp.bfloat16
 VMEM = pl.BlockSpec(memory_space=pltpu.VMEM)
@@ -75,19 +76,15 @@
     return jnp.concatenate([rows[:, k * 128 : (k + 1) * 128] for k in range(SUB)], axis=0)
 
 
-def tile_rows(rows, scratch, out_hbm, sems):
-    copies = []
-    for part in range(3):
-        groups = range(part * 4, part * 4 + 4)
-        wide = jnp.concatenate([stack_blocks(rows[g * 16 : (g + 1) * 16]) for g in groups], axis=1)
-        tiled = dot(swap_matrix(), wide).astype(BF16)
-        for i, g in enumerate(groups):
-            scratch[g * 256 : (g + 1) * 256, :] = tiled[:, i * 128 : (i + 1) * 128]
-        here = pl.ds(part * 1024, 1024)
-        copies.append(pltpu.make_async_copy(scratch.at[here, :], out_hbm.at[here, :], sems.at[part]))
-        copies[-1].start()
-    for copy in copies:
-        copy.wait()
+def tile_rows(rows, groups, scratch, out_hbm, sem):
+    wide = jnp.concatenate([stack_blocks(rows[i * 16 : (i + 1) * 16]) for i in range(len(groups))], axis=1)
+    tiled = dot(swap_matrix(), wide).astype(BF16)
+    for i, g in enumerate(groups):
+        scratch[g * 256 : (g + 1) * 256, :] = tiled[:, i * 128 : (i + 1) * 128]
+    here = pl.ds(groups[0] * 256, len(groups) * 256)
+    copy = pltpu.make_async_copy(scratch.at[here, :], out_hbm.at[here, :], sem)
+    copy.start()
+    return copy
 
 
 def untile_groups(in_ref, groups, place):
@@ -139,7 +136,13 @@
     x = x_ref[...].astype(F32)
     scale = lax.rsqrt(jnp.mean(x * x, axis=-1, keepdims=True) + 1e-06)
     normed = (x * scale * gain_ref[...].astype(F32).reshape(1, D)).astype(BF16)
-    tile_rows(dot(select, normed).astype(BF16), scratch, out_hbm, sems)
+    sent = dot(select, normed).astype(BF16)
+    copies = [
+        tile_rows(sent[part * 64 : (part + 1) * 64], range(part * 4, part * 4 + 4), scratch, out_hbm, sems.at[part])
+        for part in range(3)
+    ]
+    for copy in copies:
+        copy.wait()
 
 
 def prep(tp, routed_input, gain, routes):
@@ -196,19 +199,19 @@
     upper = dot(x, up_ref[0])
     hidden = (gate / (1.0 + jnp.exp(-gate)) * upper).astype(BF16)
     result = dot(hidden, down_ref[0]).astype(BF16)
-    rows = result.shape[0] // count
-    for i, out in enumerate(outs):
-        out[...] = result[i * rows : (i + 1) * rows]
-
-
-def expert_rows(weights, places, *blocks):
+    at = 0
+    for out in outs:
+        out[...] = result[at : at + out.shape[0]]
+        at += out.shape[0]
+
+
+def expert_rows(weights, pieces, *blocks):
     rows = sum(b.shape[0] for b in blocks)
-    count = len(places)
-    return pl.pallas_call(
-        functools.partial(rows_kernel, count),
-        out_shape=[place((rows // count, D), BF16) for place in places],
+    return pl.pallas_call(
+        functools.partial(rows_kernel, len(pieces)),
+        out_shape=[place((count, D), BF16) for count, place in pieces],
         in_specs=[VMEM] * (len(blocks) + 3),
-        out_specs=[VMEM] * count,
+        out_specs=[VMEM] * len(pieces),
         cost_estimate=cost(3_000_000 * rows, 8_000 * rows),
         name="expert_rows",
         compiler_params=LIMIT,
@@ -223,34 +226,62 @@
 def add_pairs(kept_a, came_a, kept_b, came_b):
     return pl.pallas_call(
         add_kernel,
-        out_shape=[near_out((TOP, D))] * 2,
+        out_shape=[near_out((QUARTER, D))] * 2,
         in_specs=[VMEM] * 4,
         out_specs=[VMEM] * 2,
-        cost_estimate=cost(10_000_000, 2_400_000),
+        cost_estimate=cost(10_000_000, 1_200_000),
         name="add_pairs",
         compiler_params=LIMIT,
     )(kept_a, near(came_a), kept_b, near(came_b))
 
 
-def total_kernel(own_ref, a0_ref, b0_ref, a1_ref, b1_ref, out_hbm, scratch, sems):
-    added = [
-        own_ref[i * TOP : (i + 1) * TOP, :].astype(F32) + (a_ref[...].astype(F32) + b_ref[...].astype(F32))
-        for i, (a_ref, b_ref) in enumerate(((a0_ref, b0_ref), (a1_ref, b1_ref)))
-    ]
-    tile_rows(jnp.concatenate(added, axis=0).astype(BF16), scratch, out_hbm, sems)
-
-
-def total(*parts):
-    return pl.pallas_call(
-        total_kernel,
+def total1_kernel(own_ref, top_ref, bottom_ref, top1_ref, bottom1_ref, out_hbm, sum_ref, scratch, sems):
+    copies = []
+    for half, (early, late) in enumerate(((top_ref, top1_ref), (bottom_ref, bottom1_ref))):
+        first = slice(half * TOP, half * TOP + QUARTER)
+        second = slice(half * TOP + QUARTER, (half + 1) * TOP)
+        added = own_ref[first, :].astype(F32) + (early[:QUARTER, :].astype(F32) + late[...].astype(F32))
+        copies.append(tile_rows(added.astype(BF16), range(half * 6, half * 6 + 3), scratch, out_hbm, sems.at[half]))
+        sum_ref[half] = own_ref[second, :].astype(F32) + early[QUARTER:, :].astype(F32)
+    for copy in copies:
+        copy.wait()
+
+
+def total1(*parts):
+    return pl.pallas_call(
+        total1_kernel,
+        out_shape=[pltpu.HBM((SLOTS * SUB, 128), BF16), near_out((2, QUARTER, D), F32)],
+        in_specs=[VMEM] * 5,
+        out_specs=[HBM, VMEM],
+        scratch_shapes=TILES,
+        cost_estimate=cost(200_000_000, 3_000_000),
+        name="total1",
+        compiler_params=LIMIT,
+    )(parts[0], *(near(p) for p in parts[1:]))
+
+
+def total2_kernel(begun_hbm, sum_ref, top2_ref, bottom2_ref, out_hbm, scratch, sems):
+    copies = []
+    for half, late in enumerate((top2_ref, bottom2_ref)):
+        added = sum_ref[half] + late[...].astype(F32)
+        groups = range(half * 6 + 3, half * 6 + 6)
+        copies.append(tile_rows(added.astype(BF16), groups, scratch, out_hbm, sems.at[half]))
+    for copy in copies:
+        copy.wait()
+
+
+def total2(begun, *parts):
+    return pl.pallas_call(
+        total2_kernel,
         out_shape=pltpu.HBM((SLOTS * SUB, 128), BF16),
-        in_specs=[VMEM] * 5,
+        in_specs=[HBM] + [VMEM] * 3,
         out_specs=HBM,
         scratch_shapes=TILES,
-        cost_estimate=cost(400_000_000, 3_000_000),
-        name="total",
-        compiler_params=LIMIT,
-    )(parts[0], *(near(p) for p in parts[1:]))
+        input_output_aliases={0: 0},
+        cost_estimate=cost(200_000_000, 1_500_000),
+        name="total2",
+        compiler_params=LIMIT,
+    )(begun, *(near(p) for p in parts))
 
 
 def combine_kernel(tp_ref, r_ref, route_ref, weight_ref, o_ref, plain):
@@ -452,19 +483,23 @@
     right_top = lax.ppermute(own_top, "tp", tp_perm(-1))
     far_top = lax.ppermute(left_top, "tp", tp_perm(1))
     far_bottom = lax.ppermute(right_bottom, "tp", tp_perm(-1))
-    (own_part,) = expert_rows(weights, (pltpu.HBM,), own_top, own_bottom)
-    left_part_top, left_part_bottom, right_part_top, right_part_bottom = expert_rows(
-        weights, (pltpu.VMEM, pltpu.HBM, pltpu.HBM, pltpu.VMEM), left_top, left_bottom, right_top, right_bottom
+    quarter, half = (QUARTER, pltpu.HBM), (TOP, pltpu.VMEM)
+    (own_part,) = expert_rows(weights, ((SLOTS, pltpu.HBM),), own_top, own_bottom)
+    left_early, left1, left2, right1, right2, right_early = expert_rows(
+        weights, (half, quarter, quarter, quarter, quarter, half), left_top, left_bottom, right_top, right_bottom
     )
-    far_part_top, far_part_bottom = expert_rows(weights, (pltpu.VMEM,) * 2, far_top, far_bottom)
-    from_right_top = lax.ppermute(left_part_top, "tp", tp_perm(-1))
-    from_left_bottom = lax.ppermute(right_part_bottom, "tp", tp_perm(1))
-    passed_top = lax.ppermute(far_part_top, "tp", tp_perm(1))
-    passed_bottom = lax.ppermute(far_part_bottom, "tp", tp_perm(-1))
-    right_part_top, left_part_bottom = add_pairs(right_part_top, passed_top, left_part_bottom, passed_bottom)
-    from_left_top = lax.ppermute(right_part_top, "tp", tp_perm(1))
-    from_right_bottom = lax.ppermute(left_part_bottom, "tp", tp_perm(-1))
-    mine = total(own_part, from_right_top, from_left_top, from_left_bottom, from_right_bottom)
+    top1, top2, bottom1, bottom2 = expert_rows(weights, ((QUARTER, pltpu.VMEM),) * 4, far_top, far_bottom)
+    early_top = lax.ppermute(left_early, "tp", tp_perm(-1))
+    early_bottom = lax.ppermute(right_early, "tp", tp_perm(1))
+    late = []
+    for top, bottom, left, right in ((top1, bottom1, left1, right1), (top2, bottom2, left2, right2)):
+        passed_top = lax.ppermute(top, "tp", tp_perm(1))
+        passed_bottom = lax.ppermute(bottom, "tp", tp_perm(-1))
+        right, left = add_pairs(right, passed_top, left, passed_bottom)
+        late.append((lax.ppermute(right, "tp", tp_perm(1)), lax.ppermute(left, "tp", tp_perm(-1))))
+    (late_top1, late_bottom1), (late_top2, late_bottom2) = late
+    mine, sums = total1(own_part, early_top, early_bottom, late_top1, late_bottom1)
+    mine = total2(mine, sums, late_top2, late_bottom2)
     expert_out = combine(tp, over_experts(mine), routes, route_weight)
 
     same, other = gather_kv(key_cache, value_cache)

time: 138 us -> 144 us (1.043)
  starting transfers between devices: 53.2 us -> 60.1 us
  waiting for transfers between devices: 63.4 us -> 59.8 us
  local copies, waits for them, and re-layouts: 3.18 us -> 4.88 us
    ppermute x6 -> x10, waiting for transfers between devices: 12.8 us -> 6.4 us  [the longest x2 5.95 us: body(): passed_bottom = lax.ppermute(bottom, 'tp', tp_perm(-1))]
    ppermute x6 -> x10, starting transfers between devices: 7.89 us -> 12.9 us  [the longest x2 6.14 us: body(): lax.ppermute(left, 'tp', tp_perm(-1))]
    ppermute x1, waiting for transfers between devices: 4.74 us -> 7.4 us  [body(): left_bottom = lax.ppermute(own_bottom, 'tp', tp_perm(1))]
    all_to_all x2, starting transfers between devices: 24 us -> 26.1 us  [over_experts(): lax.all_to_all(x.reshape(EXPERTS, 48, 128), 'ep', 0, 0, tiled=True)]
    unnamed x26 -> x30, local copies, waits for them, and re-layouts: 3.18 us -> 4.88 us
    pallas_call x5 -> x7, Pallas kernels: 6.52 us -> 7.34 us  [the longest x3 4.97 us: expert_rows(): pl.pallas_call(functools.partial(rows_kernel, len(pieces)), out_shape=[pl...]
  transfers between devices with their start and end apart: 22 -> 26, of which waited for: 14 -> 12; matrix products, arithmetic and copies ran while one was open for 0% -> 0% of each run, Pallas kernels for 9% -> 10%
where the time goes in v3:
time: 144 us
  starting transfers between devices  60.1 us (42%)
  waiting for transfers between devices  59.8 us (42%)
  Pallas kernels  17.9 us (12%)
  local copies, waits for them, and re-layouts  4.88 us (3%)
    all_to_all x2, starting transfers between devices, over_experts(): lax.all_to_all(x.reshape(EXPERTS, 48, 128), 'ep', 0, 0, tiled=True)  26.1 us
    all_to_all x2, waiting for transfers between devices, over_experts(): lax.all_to_all(x.reshape(EXPERTS, 48, 128), 'ep', 0, 0, tiled=True)  25.2 us
    ppermute x1, waiting for transfers between devices, body(): left_top = lax.ppermute(own_top, 'tp', tp_perm(1))  8.61 us
    ppermute x1, waiting for transfers between devices, body(): left_bottom = lax.ppermute(own_bottom, 'tp', tp_perm(1))  7.4 us
    ppermute x2, starting transfers between devices, body(): lax.ppermute(left, 'tp', tp_perm(-1))  6.14 us
    ppermute x2, waiting for transfers between devices, body(): passed_bottom = lax.ppermute(bottom, 'tp', tp_perm(-1))  5.95 us
    ppermute x1, waiting for transfers between devices, body(): far_top = lax.ppermute(left_top, 'tp', tp_perm(1))  5.07 us
    pallas_call x3, Pallas kernels, expert_rows(): pl.pallas_call(functools.partial(rows_kernel, len(pieces)), out_shape=[pl...  4.97 us
  transfers between devices with their start and end apart: 26, of which 12 were waited for; matrix products, arithmetic and copies ran while one was open for 0% of the time, Pallas kernels for 10%

profile of v3, /device:TPU:1, one launch (start us, length us, event | category | flops | bytes accessed | tf_op | source)
XLA Modules:
  0.0 143.6 jit_solution(4751881068444282417)
XLA Ops:
  0.7 2.6 %prep.1 = bf16[3072,128]{1,0:T(8,128)(2,1)} custom-call(s32[1]{0:T(128)} %bitcast.tp_ref, bf16[256,2048]{1,0:T(8,128)(2,1)} %x_hbm.1, bf16[2048]{0:T(1024)(128)(2,1)} %gain_hbm.1, s32[2,256]{1,0:T(2,128)} %bitcast.12), custom_call_target="tpu_custom_call" | custom-call | flops 400000000 | bytes 2000000 | tf_op jit(solution)/shard_map/prep/pallas_call | solution.py:149
  3.3 13.3 %all-to-all-start.1 = ((bf16[64,48,128]{2,1,0:T(8,128)(2,1)}), bf16[64,48,128]{2,1,0:T(8,128)(2,1)}, u32[]{:S(2)}, u32[]{:S(2)}) async-start(bf16[64,48,128]{2,1,0:T(8,128)(2,1)} %bitcast.15), calls=%async_computation.1 | async-start | bytes 1572864 | tf_op jit(solution)/shard_map/all_to_all | solution.py:427
  16.7 1.4 collective-permute-start
  18.1 1.3 collective-permute-start.1
  19.4 1.6 %collective-permute-start.2 = (bf16[128,128]{1,0:T(8,128)(2,1)S(1)}, bf16[128,128]{1,0:T(8,128)(2,1)S(1)}, u32[]{:S(2)}, u32[]{:S(2)}) collective-permute-start(bf16[128,128]{1,0:T(8,128)(2,1)S(1)} %pad_maximum_fusion.a_ref), channel_id=1, source_target_pairs={{0,16},{4,20},{8,24},{12,28},{16,0},{20,4},{24,8},{28,12},{32,48},... | collective-permute-start | bytes 98312 | tf_op jit(solution)/shard_map/ppermute | solution.py:455
  21.1 0.7 collective-permute-done.b_ref
  21.8 2.4 %collective-permute-done.2.d_ref = bf16[128,128]{1,0:T(8,128)(2,1)S(1)} collective-permute-done((bf16[128,128]{1,0:T(8,128)(2,1)S(1)}, bf16[128,128]{1,0:T(8,128)(2,1)S(1)}, u32[]{:S(2)}, u32[]{:S(2)}) %collective-permute-start.2) | collective-permute-done | bytes 32800 | tf_op jit(solution)/shard_map/ppermute | solution.py:455
  24.1 1.1 repeat.1
  25.3 14.3 %all-to-all-done.1 = bf16[64,48,128]{2,1,0:T(8,128)(2,1)} async-done(((bf16[64,48,128]{2,1,0:T(8,128)(2,1)}), bf16[64,48,128]{2,1,0:T(8,128)(2,1)}, u32[]{:S(2)}, u32[]{:S(2)}) %all-to-all-start.1) | async-done | bytes 786464 | tf_op jit(solution)/shard_map/all_to_all | solution.py:427
  39.5 4.2 %all-to-all-start = ((bf16[8,4,128,128]{3,2,1,0:T(8,128)(2,1)}), bf16[8,4,128,128]{3,2,1,0:T(8,128)(2,1)}, u32[]{:S(2)}, u32[]{:S(2)}) async-start(bf16[8,4,128,128]{3,2,1,0:T(8,128)(2,1)} %repeat.1), calls=%async_computation | async-start | bytes 2097152 | tf_op jit(solution)/shard_map/all_to_all | solution.py:449
  43.8 1.7 %untile.1 = (bf16[96,2048]{1,0:T(8,128)(2,1)S(1)}, bf16[96,2048]{1,0:T(8,128)(2,1)S(1)}) custom-call(bf16[3072,128]{1,0:T(8,128)(2,1)} %bitcast.7.a_hbm), custom_call_target="tpu_custom_call" | custom-call | flops 400000000 | bytes 1600000 | tf_op jit(solution)/shard_map/untile/pallas_call | solution.py:183
  45.5 1.3 collective-permute-start.7
  46.8 1.5 %collective-permute-start.10 = (bf16[96,2048]{1,0:T(8,128)(2,1)S(1)}, bf16[96,2048]{1,0:T(8,128)(2,1)S(1)}, u32[]{:S(2)}, u32[]{:S(2)}) collective-permute-start(bf16[96,2048]{1,0:T(8,128)(2,1)S(1)} %get-tuple-element.35.refs_1_), channel_id=1, source_target_pairs={{0,3},{1,0},{2,1},{3,2},{4,7},{5,4},{6,5},{7,6},{8,11},{9,8},{10,9... | collective-permute-start | bytes 1179656 | tf_op jit(solution)/shard_map/ppermute | solution.py:481
  48.2 8.6 %collective-permute-done.7.refs_0_ = bf16[96,2048]{1,0:T(8,128)(2,1)S(1)} collective-permute-done((bf16[96,2048]{1,0:T(8,128)(2,1)S(1)}, bf16[96,2048]{1,0:T(8,128)(2,1)S(1)}, u32[]{:S(2)}, u32[]{:S(2)}) %collective-permute-start.7) | collective-permute-done | bytes 393248 | tf_op jit(solution)/shard_map/ppermute | solution.py:480
  56.9 2.7 %collective-permute-start.14 = (bf16[96,2048]{1,0:T(8,128)(2,1)S(1)}, bf16[96,2048]{1,0:T(8,128)(2,1)S(1)}, u32[]{:S(2)}, u32[]{:S(2)}) collective-permute-start(bf16[96,2048]{1,0:T(8,128)(2,1)S(1)} %collective-permute-done.10.refs_3_), channel_id=1, source_target_pairs={{0,3},{1,0},{2,1},{3,2},{4,7},{5,4},{6,5},{7,6},{8,11},{9,8},{10,9... | collective-permute-start | bytes 1179656 | tf_op jit(solution)/shard_map/ppermute | solution.py:485
  59.5 2.7 %collective-permute-start.9 = (bf16[96,2048]{1,0:T(8,128)(2,1)S(1)}, bf16[96,2048]{1,0:T(8,128)(2,1)S(1)}, u32[]{:S(2)}, u32[]{:S(2)}) collective-permute-start(bf16[96,2048]{1,0:T(8,128)(2,1)S(1)} %get-tuple-element.34.refs_0_), channel_id=1, source_target_pairs={{0,3},{1,0},{2,1},{3,2},{4,7},{5,4},{6,5},{7,6},{8,11},{9,8},{10,9... | collective-permute-start | bytes 1179656 | tf_op jit(solution)/shard_map/ppermute | solution.py:483
  62.2 5.1 %collective-permute-done.13.refs_0_ = bf16[96,2048]{1,0:T(8,128)(2,1)S(1)} collective-permute-done((bf16[96,2048]{1,0:T(8,128)(2,1)S(1)}, bf16[96,2048]{1,0:T(8,128)(2,1)S(1)}, u32[]{:S(2)}, u32[]{:S(2)}) %collective-permute-start.13) | collective-permute-done | bytes 393248 | tf_op jit(solution)/shard_map/ppermute | solution.py:484
  67.3 0.9 expert_rows.5
  68.3 7.4 %collective-permute-done.8.refs_1_ = bf16[96,2048]{1,0:T(8,128)(2,1)S(1)} collective-permute-done((bf16[96,2048]{1,0:T(8,128)(2,1)S(1)}, bf16[96,2048]{1,0:T(8,128)(2,1)S(1)}, u32[]{:S(2)}, u32[]{:S(2)}) %collective-permute-start.8) | collective-permute-done | bytes 393248 | tf_op jit(solution)/shard_map/ppermute | solution.py:482
  75.7 2.3 %expert_rows.4 = (bf16[96,2048]{1,0:T(8,128)(2,1)S(1)}, bf16[48,2048]{1,0:T(8,128)(2,1)}, bf16[48,2048]{1,0:T(8,128)(2,1)}, bf16[48,2048]{1,0:T(8,128)(2,1)}, bf...) custom-call(bf16[96,2048]{1,0:T(8,128)(2,1)S(1)} %collective-permute-done.7.refs_0_, ...), custom_call_target="tpu_custom_call" | custom-call | flops 1152000000 | bytes 3072000 | tf_op jit(solution)/shard_map/expert_rows/pallas_call | solution.py:210
  78.0 2.4 %collective-permute-start.11 = (bf16[96,2048]{1,0:T(8,128)(2,1)S(1)}, bf16[96,2048]{1,0:T(8,128)(2,1)S(1)}, u32[]{:S(2)}, u32[]{:S(2)}) collective-permute-start(bf16[96,2048]{1,0:T(8,128)(2,1)S(1)} %get-tuple-element.36), channel_id=1, source_target_pairs={{0,3},{1,0},{2,1},{3,2},{4,7},{5,4},{6,5},{7,6},{8,11},{9,8},{10,9... | collective-permute-start | bytes 1179656 | tf_op jit(solution)/shard_map/ppermute | solution.py:492
  80.4 1.4 %collective-permute-start.19 = (bf16[48,2048]{1,0:T(8,128)(2,1)S(1)}, bf16[48,2048]{1,0:T(8,128)(2,1)S(1)}, u32[]{:S(2)}, u32[]{:S(2)}) collective-permute-start(bf16[48,2048]{1,0:T(8,128)(2,1)S(1)} %get-tuple-element.47), channel_id=1, source_target_pairs={{0,1},{1,2},{2,3},{3,0},{4,5},{5,6},{6,7},{7,4},{8,9},{9,10},{10,1... | collective-permute-start | bytes 589832 | tf_op jit(solution)/shard_map/ppermute | solution.py:496
  81.9 2.7 %collective-permute-start.20 = (bf16[48,2048]{1,0:T(8,128)(2,1)S(1)}, bf16[48,2048]{1,0:T(8,128)(2,1)S(1)}, u32[]{:S(2)}, u32[]{:S(2)}) collective-permute-start(bf16[48,2048]{1,0:T(8,128)(2,1)S(1)} %get-tuple-element.49), channel_id=1, source_target_pairs={{0,3},{1,0},{2,1},{3,2},{4,7},{5,4},{6,5},{7,6},{8,11},{9,8},{10,9... | collective-permute-start | bytes 589832 | tf_op jit(solution)/shard_map/ppermute | solution.py:497
  84.5 6.0 %collective-permute-done.16.d_ref = bf16[48,2048]{1,0:T(8,128)(2,1)S(1)} collective-permute-done((bf16[48,2048]{1,0:T(8,128)(2,1)S(1)}, bf16[48,2048]{1,0:T(8,128)(2,1)S(1)}, u32[]{:S(2)}, u32[]{:S(2)}) %collective-permute-start.16) | collective-permute-done | bytes 196640 | tf_op jit(solution)/shard_map/ppermute | solution.py:497
  90.5 0.9 copy-done.7
  91.4 0.9 copy-done.8
  92.3 0.1 add_pairs.2
  92.5 3.5 %collective-permute-start.18 = (bf16[48,2048]{1,0:T(8,128)(2,1)S(1)}, bf16[48,2048]{1,0:T(8,128)(2,1)S(1)}, u32[]{:S(2)}, u32[]{:S(2)}) collective-permute-start(bf16[48,2048]{1,0:T(8,128)(2,1)S(1)} %get-tuple-element.43), channel_id=1, source_target_pairs={{0,3},{1,0},{2,1},{3,2},{4,7},{5,4},{6,5},{7,6},{8,11},{9,8},{10,9... | collective-permute-start | bytes 589832 | tf_op jit(solution)/shard_map/ppermute | solution.py:499
  96.0 0.9 copy-done.5
  96.9 0.9 copy-done.6
  98.1 2.7 %collective-permute-start.22 = (bf16[48,2048]{1,0:T(8,128)(2,1)S(1)}, bf16[48,2048]{1,0:T(8,128)(2,1)S(1)}, u32[]{:S(2)}, u32[]{:S(2)}) collective-permute-start(bf16[48,2048]{1,0:T(8,128)(2,1)S(1)} %get-tuple-element.51), channel_id=1, source_target_pairs={{0,3},{1,0},{2,1},{3,2},{4,7},{5,4},{6,5},{7,6},{8,11},{9,8},{10,9... | collective-permute-start | bytes 589832 | tf_op jit(solution)/shard_map/ppermute | solution.py:499
  100.7 1.8 %expert_rows.3.own_ref = bf16[192,2048]{1,0:T(8,128)(2,1)} custom-call(bf16[96,2048]{1,0:T(8,128)(2,1)S(1)} %get-tuple-element.34.refs_0_, bf16[96,2048]{1,0:T(8,128)(2,1)S(1)} %get-tuple-element.35.refs_1_, bf16[1,2048,256]{2,1,0:T(8,128)(2,1)S(1)} %copy-done, bf16[1,2048,256]{2,1,0:T(8,128)(2,1)S(1)} %copy-done.1, bf16[1,256,2048]{2,1,0:T(8,128)(2,1)S(1)} %copy-done.2), custom_call_target="tpu_custom_call" | custom-call | flops 576000000 | bytes 1536000 | tf_op jit(solution)/shard_map/expert_rows/pallas_call | solution.py:210
  102.5 1.1 copy-done.3
  103.7 1.1 total1.1
  104.8 0.4 collective-permute-done.21.top2_ref
  105.3 1.0 total2.1
  106.3 12.8 %all-to-all-start.2 = ((bf16[64,48,128]{2,1,0:T(8,128)(2,1)}), bf16[64,48,128]{2,1,0:T(8,128)(2,1)S(1)}, u32[]{:S(2)}, u32[]{:S(2)}) async-start(bf16[64,48,128]{2,1,0:T(8,128)(2,1)} %bitcast.16), calls=%async_computation.2 | async-start | bytes 1572864 | tf_op jit(solution)/shard_map/all_to_all | solution.py:427
  119.1 0.5 collective-permute-start.3
  119.7 1.7 %attend_same.1 = (f32[256,1]{1,0:T(8,128)S(1)}, f32[256,1]{1,0:T(8,128)S(1)}, f32[256,64]{1,0:T(8,128)S(1)}) custom-call(s32[1]{0:T(128)} %bitcast.1.ep_ref, s32[1]{0:T(128)} %bitcast.tp_ref, bf16[128,128]{1,0:T(8,128)(2,1)S(1)} %copy-done.10, f32[1,8192]{1,0:T(1,128)S(1)} %copy-done.11, bf16[32,128,128]{2,1,0:T(8,128)(2,1)} %bitcast.4.blocks_ref), custom_call_target="tpu_custom_call" | custom-call | flops 2000000000 | bytes 1500000 | tf_op jit(solution)/shard_map/attend_same/pallas_call | solution.py:381
  121.4 0.8 collective-permute-done.3.blocks_ref
  122.2 0.9 attend_other.1
  123.2 2.7 %collective-permute-start.5 = (bf16[32,128]{1,0:T(8,128)(2,1)S(1)}, bf16[32,128]{1,0:T(8,128)(2,1)S(1)}, u32[]{:S(2)}, u32[]{:S(2)}) collective-permute-start(bf16[32,128]{1,0:T(8,128)(2,1)S(1)} %get-tuple-element.32), channel_id=1, source_target_pairs={{0,3},{1,0},{2,1},{3,2},{4,7},{5,4},{6,5},{7,6},{8,11},{9,8},{10,9... | collective-permute-start | bytes 24584 | tf_op jit(solution)/shard_map/ppermute | solution.py:511
  125.8 1.0 collective-permute-start.6
  126.8 0.4 collective-permute-done.4.b_ref
  127.2 3.0 %collective-permute-done.6.d_ref = bf16[32,128]{1,0:T(8,128)(2,1)S(1)} collective-permute-done((bf16[32,128]{1,0:T(8,128)(2,1)S(1)}, bf16[32,128]{1,0:T(8,128)(2,1)S(1)}, u32[]{:S(2)}, u32[]{:S(2)}) %collective-permute-start.6) | collective-permute-done | bytes 8224 | tf_op jit(solution)/shard_map/ppermute | solution.py:512
  130.1 1.1 project.1
  131.2 10.9 %all-to-all-done.2 = bf16[64,48,128]{2,1,0:T(8,128)(2,1)S(1)} async-done(((bf16[64,48,128]{2,1,0:T(8,128)(2,1)}), bf16[64,48,128]{2,1,0:T(8,128)(2,1)S(1)}, u32[]{:S(2)}, u32[]{:S(2)}) %all-to-all-start.2) | async-done | bytes 786464 | tf_op jit(solution)/shard_map/all_to_all | solution.py:427
  142.2 1.4 %combine.1 = bf16[64,2048]{1,0:T(8,128)(2,1)} custom-call(s32[1]{0:T(128)} %bitcast.tp_ref, bf16[3072,128]{1,0:T(8,128)(2,1)S(1)} %bitcast.11, s32[2,256]{1,0:T(2,128)S(1)} %bitcast.13, f32[2,256]{1,0:T(2,128)S(1)} %bitcast.14), custom_call_target="tpu_custom_call" | custom-call | flops 400000000 | bytes 2000000 | tf_op jit(solution)/shard_map/combine/pallas_call | solution.py:303
  (49 shorter events, 0.6 us)
Async XLA Ops:
  0.6 16.0 %copy-start.14 = (bf16[1,64,128]{2,1,0:T(8,128)(2,1)S(1)}, bf16[1,64,128]{2,1,0:T(8,128)(2,1)}, u32[]{:S(2)}) copy-start(bf16[1,64,128]{2,1,0:T(8,128)(2,1)} %param.13) | copy-start | bytes 49156
  0.6 16.0 %copy-start.13 = (bf16[1,64,128]{2,1,0:T(8,128)(2,1)S(1)}, bf16[1,64,128]{2,1,0:T(8,128)(2,1)}, u32[]{:S(2)}) copy-start(bf16[1,64,128]{2,1,0:T(8,128)(2,1)} %param.14) | copy-start | bytes 49156
  3.3 36.3 %all-to-all-start.1 = ((bf16[64,48,128]{2,1,0:T(8,128)(2,1)}), bf16[64,48,128]{2,1,0:T(8,128)(2,1)}, u32[]{:S(2)}, u32[]{:S(2)}) async-start(bf16[64,48,128]{2,1,0:T(8,128)(2,1)} %bitcast.15), calls=%async_computation.1 | async-start | bytes 1572864 | tf_op jit(solution)/shard_map/all_to_all | solution.py:427
  16.6 50.6 %copy-start = (bf16[1,2048,256]{2,1,0:T(8,128)(2,1)S(1)}, bf16[1,2048,256]{2,1,0:T(8,128)(2,1)}, u32[]{:S(2)}) copy-start(bf16[1,2048,256]{2,1,0:T(8,128)(2,1)} %refs_2_.3) | copy-start | bytes 3145732
  16.7 50.6 %copy-start.1 = (bf16[1,2048,256]{2,1,0:T(8,128)(2,1)S(1)}, bf16[1,2048,256]{2,1,0:T(8,128)(2,1)}, u32[]{:S(2)}) copy-start(bf16[1,2048,256]{2,1,0:T(8,128)(2,1)} %refs_3_.3) | copy-start | bytes 3145732
  16.7 50.6 %copy-start.2 = (bf16[1,256,2048]{2,1,0:T(8,128)(2,1)S(1)}, bf16[1,256,2048]{2,1,0:T(8,128)(2,1)}, u32[]{:S(2)}) copy-start(bf16[1,256,2048]{2,1,0:T(8,128)(2,1)} %refs_4_.5) | copy-start | bytes 3145732
  16.7 5.1 %collective-permute-start = (bf16[128,128]{1,0:T(8,128)(2,1)S(1)}, bf16[128,128]{1,0:T(8,128)(2,1)S(1)}, u32[]{:S(2)}, u32[]{:S(2)}) collective-permute-start(bf16[128,128]{1,0:T(8,128)(2,1)S(1)} %pad_maximum_fusion.a_ref), channel_id=1, source_target_pairs={{0,8},{4,12},{8,16},{12,20},{16,24},{20,28},{24,0},{28,4},{32,40},... | collective-permute-start | bytes 98312 | tf_op jit(solution)/shard_map/ppermute | solution.py:455
  18.1 3.7 %collective-permute-start.1 = (bf16[128,128]{1,0:T(8,128)(2,1)S(1)}, bf16[128,128]{1,0:T(8,128)(2,1)S(1)}, u32[]{:S(2)}, u32[]{:S(2)}) collective-permute-start(bf16[128,128]{1,0:T(8,128)(2,1)S(1)} %pad_maximum_fusion.a_ref), channel_id=1, source_target_pairs={{0,24},{4,28},{8,0},{12,4},{16,8},{20,12},{24,16},{28,20},{32,56},... | collective-permute-start | bytes 98312 | tf_op jit(solution)/shard_map/ppermute | solution.py:455
  19.4 4.7 %collective-permute-start.2 = (bf16[128,128]{1,0:T(8,128)(2,1)S(1)}, bf16[128,128]{1,0:T(8,128)(2,1)S(1)}, u32[]{:S(2)}, u32[]{:S(2)}) collective-permute-start(bf16[128,128]{1,0:T(8,128)(2,1)S(1)} %pad_maximum_fusion.a_ref), channel_id=1, source_target_pairs={{0,16},{4,20},{8,24},{12,28},{16,0},{20,4},{24,8},{28,12},{32,48},... | collective-permute-start | bytes 98312 | tf_op jit(solution)/shard_map/ppermute | solution.py:455
  39.5 66.8 %all-to-all-start = ((bf16[8,4,128,128]{3,2,1,0:T(8,128)(2,1)}), bf16[8,4,128,128]{3,2,1,0:T(8,128)(2,1)}, u32[]{:S(2)}, u32[]{:S(2)}) async-start(bf16[8,4,128,128]{3,2,1,0:T(8,128)(2,1)} %repeat.1), calls=%async_computation | async-start | bytes 2097152 | tf_op jit(solution)/shard_map/all_to_all | solution.py:449
  45.5 11.4 %collective-permute-start.7 = (bf16[96,2048]{1,0:T(8,128)(2,1)S(1)}, bf16[96,2048]{1,0:T(8,128)(2,1)S(1)}, u32[]{:S(2)}, u32[]{:S(2)}) collective-permute-start(bf16[96,2048]{1,0:T(8,128)(2,1)S(1)} %get-tuple-element.34.refs_0_), channel_id=1, source_target_pairs={{0,1},{1,2},{2,3},{3,0},{4,5},{5,6},{6,7},{7,4},{8,9},{9,10},{10,1... | collective-permute-start | bytes 1179656 | tf_op jit(solution)/shard_map/ppermute | solution.py:480
  46.8 10.1 %collective-permute-start.10 = (bf16[96,2048]{1,0:T(8,128)(2,1)S(1)}, bf16[96,2048]{1,0:T(8,128)(2,1)S(1)}, u32[]{:S(2)}, u32[]{:S(2)}) collective-permute-start(bf16[96,2048]{1,0:T(8,128)(2,1)S(1)} %get-tuple-element.35.refs_1_), channel_id=1, source_target_pairs={{0,3},{1,0},{2,1},{3,2},{4,7},{5,4},{6,5},{7,6},{8,11},{9,8},{10,9... | collective-permute-start | bytes 1179656 | tf_op jit(solution)/shard_map/ppermute | solution.py:481
  56.9 10.4 %collective-permute-start.13 = (bf16[96,2048]{1,0:T(8,128)(2,1)S(1)}, bf16[96,2048]{1,0:T(8,128)(2,1)S(1)}, u32[]{:S(2)}, u32[]{:S(2)}) collective-permute-start(bf16[96,2048]{1,0:T(8,128)(2,1)S(1)} %collective-permute-done.7.refs_0_), channel_id=1, source_target_pairs={{0,1},{1,2},{2,3},{3,0},{4,5},{5,6},{6,7},{7,4},{8,9},{9,10},{10,1... | collective-permute-start | bytes 1179656 | tf_op jit(solution)/shard_map/ppermute | solution.py:484
  56.9 10.4 %collective-permute-start.14 = (bf16[96,2048]{1,0:T(8,128)(2,1)S(1)}, bf16[96,2048]{1,0:T(8,128)(2,1)S(1)}, u32[]{:S(2)}, u32[]{:S(2)}) collective-permute-start(bf16[96,2048]{1,0:T(8,128)(2,1)S(1)} %collective-permute-done.10.refs_3_), channel_id=1, source_target_pairs={{0,3},{1,0},{2,1},{3,2},{4,7},{5,4},{6,5},{7,6},{8,11},{9,8},{10,9... | collective-permute-start | bytes 1179656 | tf_op jit(solution)/shard_map/ppermute | solution.py:485
  59.5 16.2 %collective-permute-start.8 = (bf16[96,2048]{1,0:T(8,128)(2,1)S(1)}, bf16[96,2048]{1,0:T(8,128)(2,1)S(1)}, u32[]{:S(2)}, u32[]{:S(2)}) collective-permute-start(bf16[96,2048]{1,0:T(8,128)(2,1)S(1)} %get-tuple-element.35.refs_1_), channel_id=1, source_target_pairs={{0,1},{1,2},{2,3},{3,0},{4,5},{5,6},{6,7},{7,4},{8,9},{9,10},{10,1... | collective-permute-start | bytes 1179656 | tf_op jit(solution)/shard_map/ppermute | solution.py:482
  59.5 16.2 %collective-permute-start.9 = (bf16[96,2048]{1,0:T(8,128)(2,1)S(1)}, bf16[96,2048]{1,0:T(8,128)(2,1)S(1)}, u32[]{:S(2)}, u32[]{:S(2)}) collective-permute-start(bf16[96,2048]{1,0:T(8,128)(2,1)S(1)} %get-tuple-element.34.refs_0_), channel_id=1, source_target_pairs={{0,3},{1,0},{2,1},{3,2},{4,7},{5,4},{6,5},{7,6},{8,11},{9,8},{10,9... | collective-permute-start | bytes 1179656 | tf_op jit(solution)/shard_map/ppermute | solution.py:483
  68.2 13.6 %collective-permute-start.15 = (bf16[48,2048]{1,0:T(8,128)(2,1)S(1)}, bf16[48,2048]{1,0:T(8,128)(2,1)S(1)}, u32[]{:S(2)}, u32[]{:S(2)}) collective-permute-start(bf16[48,2048]{1,0:T(8,128)(2,1)S(1)} %get-tuple-element.39), channel_id=1, source_target_pairs={{0,1},{1,2},{2,3},{3,0},{4,5},{5,6},{6,7},{7,4},{8,9},{9,10},{10,1... | collective-permute-start | bytes 589832 | tf_op jit(solution)/shard_map/ppermute | solution.py:496
  78.0 20.1 %collective-permute-start.11 = (bf16[96,2048]{1,0:T(8,128)(2,1)S(1)}, bf16[96,2048]{1,0:T(8,128)(2,1)S(1)}, u32[]{:S(2)}, u32[]{:S(2)}) collective-permute-start(bf16[96,2048]{1,0:T(8,128)(2,1)S(1)} %get-tuple-element.36), channel_id=1, source_target_pairs={{0,3},{1,0},{2,1},{3,2},{4,7},{5,4},{6,5},{7,6},{8,11},{9,8},{10,9... | collective-permute-start | bytes 1179656 | tf_op jit(solution)/shard_map/ppermute | solution.py:492
  80.4 10.1 %collective-permute-start.16 = (bf16[48,2048]{1,0:T(8,128)(2,1)S(1)}, bf16[48,2048]{1,0:T(8,128)(2,1)S(1)}, u32[]{:S(2)}, u32[]{:S(2)}) collective-permute-start(bf16[48,2048]{1,0:T(8,128)(2,1)S(1)} %get-tuple-element.41), channel_id=1, source_target_pairs={{0,3},{1,0},{2,1},{3,2},{4,7},{5,4},{6,5},{7,6},{8,11},{9,8},{10,9... | collective-permute-start | bytes 589832 | tf_op jit(solution)/shard_map/ppermute | solution.py:497
  80.4 12.1 %collective-permute-start.19 = (bf16[48,2048]{1,0:T(8,128)(2,1)S(1)}, bf16[48,2048]{1,0:T(8,128)(2,1)S(1)}, u32[]{:S(2)}, u32[]{:S(2)}) collective-permute-start(bf16[48,2048]{1,0:T(8,128)(2,1)S(1)} %get-tuple-element.47), channel_id=1, source_target_pairs={{0,1},{1,2},{2,3},{3,0},{4,5},{5,6},{6,7},{7,4},{8,9},{9,10},{10,1... | collective-permute-start | bytes 589832 | tf_op jit(solution)/shard_map/ppermute | solution.py:496
  81.8 20.7 %collective-permute-start.12 = (bf16[96,2048]{1,0:T(8,128)(2,1)S(1)}, bf16[96,2048]{1,0:T(8,128)(2,1)S(1)}, u32[]{:S(2)}, u32[]{:S(2)}) collective-permute-start(bf16[96,2048]{1,0:T(8,128)(2,1)S(1)} %get-tuple-element.37), channel_id=1, source_target_pairs={{0,1},{1,2},{2,3},{3,0},{4,5},{5,6},{6,7},{7,4},{8,9},{9,10},{10,1... | collective-permute-start | bytes 1179656 | tf_op jit(solution)/shard_map/ppermute | solution.py:493
  81.9 14.1 %collective-permute-start.20 = (bf16[48,2048]{1,0:T(8,128)(2,1)S(1)}, bf16[48,2048]{1,0:T(8,128)(2,1)S(1)}, u32[]{:S(2)}, u32[]{:S(2)}) collective-permute-start(bf16[48,2048]{1,0:T(8,128)(2,1)S(1)} %get-tuple-element.49), channel_id=1, source_target_pairs={{0,3},{1,0},{2,1},{3,2},{4,7},{5,4},{6,5},{7,6},{8,11},{9,8},{10,9... | collective-permute-start | bytes 589832 | tf_op jit(solution)/shard_map/ppermute | solution.py:497
  90.5 0.9 copy-start.7
  91.4 0.9 copy-start.8
  92.4 10.1 %collective-permute-start.17 = (bf16[48,2048]{1,0:T(8,128)(2,1)S(1)}, bf16[48,2048]{1,0:T(8,128)(2,1)S(1)}, u32[]{:S(2)}, u32[]{:S(2)}) collective-permute-start(bf16[48,2048]{1,0:T(8,128)(2,1)S(1)} %get-tuple-element.42), channel_id=1, source_target_pairs={{0,1},{1,2},{2,3},{3,0},{4,5},{5,6},{6,7},{7,4},{8,9},{9,10},{10,1... | collective-permute-start | bytes 589832 | tf_op jit(solution)/shard_map/ppermute | solution.py:499
  92.5 10.0 %collective-permute-start.18 = (bf16[48,2048]{1,0:T(8,128)(2,1)S(1)}, bf16[48,2048]{1,0:T(8,128)(2,1)S(1)}, u32[]{:S(2)}, u32[]{:S(2)}) collective-permute-start(bf16[48,2048]{1,0:T(8,128)(2,1)S(1)} %get-tuple-element.43), channel_id=1, source_target_pairs={{0,3},{1,0},{2,1},{3,2},{4,7},{5,4},{6,5},{7,6},{8,11},{9,8},{10,9... | collective-permute-start | bytes 589832 | tf_op jit(solution)/shard_map/ppermute | solution.py:499
  96.0 0.9 copy-start.5
  96.9 0.9 copy-start.6
  98.0 7.3 %collective-permute-start.21 = (bf16[48,2048]{1,0:T(8,128)(2,1)S(1)}, bf16[48,2048]{1,0:T(8,128)(2,1)S(1)}, u32[]{:S(2)}, u32[]{:S(2)}) collective-permute-start(bf16[48,2048]{1,0:T(8,128)(2,1)S(1)} %get-tuple-element.50), channel_id=1, source_target_pairs={{0,1},{1,2},{2,3},{3,0},{4,5},{5,6},{6,7},{7,4},{8,9},{9,10},{10,1... | collective-permute-start | bytes 589832 | tf_op jit(solution)/shard_map/ppermute | solution.py:499
  98.1 7.2 %collective-permute-start.22 = (bf16[48,2048]{1,0:T(8,128)(2,1)S(1)}, bf16[48,2048]{1,0:T(8,128)(2,1)S(1)}, u32[]{:S(2)}, u32[]{:S(2)}) collective-permute-start(bf16[48,2048]{1,0:T(8,128)(2,1)S(1)} %get-tuple-element.51), channel_id=1, source_target_pairs={{0,3},{1,0},{2,1},{3,2},{4,7},{5,4},{6,5},{7,6},{8,11},{9,8},{10,9... | collective-permute-start | bytes 589832 | tf_op jit(solution)/shard_map/ppermute | solution.py:499
  102.5 1.1 copy-start.3
  105.2 14.4 %copy-start.10 = (bf16[128,128]{1,0:T(8,128)(2,1)S(1)}, bf16[128,128]{1,0:T(8,128)(2,1)}, u32[]{:S(2)}) copy-start(bf16[128,128]{1,0:T(8,128)(2,1)} %q_ref.3) | copy-start | bytes 98308
  105.3 14.4 %copy-start.11 = (f32[1,8192]{1,0:T(1,128)S(1)}, f32[1,8192]{1,0:T(1,128)}, u32[]{:S(2)}) copy-start(f32[1,8192]{1,0:T(1,128)} %gate_ref.3) | copy-start | bytes 98308
  106.3 35.8 %all-to-all-start.2 = ((bf16[64,48,128]{2,1,0:T(8,128)(2,1)}), bf16[64,48,128]{2,1,0:T(8,128)(2,1)S(1)}, u32[]{:S(2)}, u32[]{:S(2)}) async-start(bf16[64,48,128]{2,1,0:T(8,128)(2,1)} %bitcast.16), calls=%async_computation.2 | async-start | bytes 1572864 | tf_op jit(solution)/shard_map/all_to_all | solution.py:427
  119.1 3.0 %collective-permute-start.3 = (bf16[32,128,128]{2,1,0:T(8,128)(2,1)}, bf16[32,128,128]{2,1,0:T(8,128)(2,1)S(1)}, u32[]{:S(2)}, u32[]{:S(2)}) collective-permute-start(bf16[32,128,128]{2,1,0:T(8,128)(2,1)} %bitcast.4.blocks_ref), channel_id=1, source_target_pairs={{0,4},{4,0},{8,12},{12,8},{16,20},{20,16},{24,28},{28,24},{32,36},... | collective-permute-start | bytes 3145736 | tf_op jit(solution)/shard_map/ppermute | solution.py:458
  122.2 8.0 %copy-start.4 = (bf16[512,2048]{1,0:T(8,128)(2,1)S(1)}, bf16[512,2048]{1,0:T(8,128)(2,1)}, u32[]{:S(2)}) copy-start(bf16[512,2048]{1,0:T(8,128)(2,1)} %w_ref.1) | copy-start | bytes 6291460
  123.1 19.1 %copy-start.9 = (s32[256,2]{0,1:T(2,128)S(1)}, s32[256,2]{0,1:T(2,128)}, u32[]{:S(2)}) copy-start(s32[256,2]{0,1:T(2,128)} %param.19) | copy-start | bytes 6148
  123.1 19.1 %copy-start.12 = (f32[256,2]{0,1:T(2,128)S(1)}, f32[256,2]{0,1:T(2,128)}, u32[]{:S(2)}) copy-start(f32[256,2]{0,1:T(2,128)} %param.20) | copy-start | bytes 6148
  123.1 4.1 %collective-permute-start.4 = (bf16[32,128]{1,0:T(8,128)(2,1)S(1)}, bf16[32,128]{1,0:T(8,128)(2,1)S(1)}, u32[]{:S(2)}, u32[]{:S(2)}) collective-permute-start(bf16[32,128]{1,0:T(8,128)(2,1)S(1)} %get-tuple-element.31), channel_id=1, source_target_pairs={{0,1},{1,2},{2,3},{3,0},{4,5},{5,6},{6,7},{7,4},{8,9},{9,10},{10,1... | collective-permute-start | bytes 24584 | tf_op jit(solution)/shard_map/ppermute | solution.py:510
  123.2 4.0 %collective-permute-start.5 = (bf16[32,128]{1,0:T(8,128)(2,1)S(1)}, bf16[32,128]{1,0:T(8,128)(2,1)S(1)}, u32[]{:S(2)}, u32[]{:S(2)}) collective-permute-start(bf16[32,128]{1,0:T(8,128)(2,1)S(1)} %get-tuple-element.32), channel_id=1, source_target_pairs={{0,3},{1,0},{2,1},{3,2},{4,7},{5,4},{6,5},{7,6},{8,11},{9,8},{10,9... | collective-permute-start | bytes 24584 | tf_op jit(solution)/shard_map/ppermute | solution.py:511
  125.8 4.3 %collective-permute-start.6 = (bf16[32,128]{1,0:T(8,128)(2,1)S(1)}, bf16[32,128]{1,0:T(8,128)(2,1)S(1)}, u32[]{:S(2)}, u32[]{:S(2)}) collective-permute-start(bf16[32,128]{1,0:T(8,128)(2,1)S(1)} %get-tuple-element.33), channel_id=1, source_target_pairs={{0,2},{1,3},{2,0},{3,1},{4,6},{5,7},{6,4},{7,5},{8,10},{9,11},{10,... | collective-permute-start | bytes 24584 | tf_op jit(solution)/shard_map/ppermute | solution.py:512
